TPU v7x, 32 devices: a whole 2x2x4 slice. The times are simulated.
32 devices in a mesh: rep: 2 (over x), fs: 8 (over z, y), tp: 2 (over core).
Axes of the slice: x: 2, y: 2, z: 4, core: 2. Of those that a mesh axis runs over, the one named last changes fastest.
Arguments:
- tokens: bfloat16 [16384, 2048], P(('rep', 'fs', 'tp')), parts along dimension 0, may hold values from -6 to 6
- mix_gain: float32 [2048], replicated, may hold values from 0.1 to 1.9
- w_query: bfloat16 [2048, 512], P('fs', 'tp'), may hold values from -0.125 to 0.125
- w_key: bfloat16 [2048, 512], P('fs', 'tp'), may hold values from -0.125 to 0.125
- w_value: bfloat16 [2048, 1024], P('fs', 'tp'), may hold values from -0.125 to 0.125
- w_out: bfloat16 [1024, 2048], P('tp', 'fs'), may hold values from -0.1875 to 0.1875
- ffn_gain: float32 [2048], replicated, may hold values from 0.1 to 1.9
- w_ffgate: bfloat16 [2048, 2816], P('fs', 'tp'), may hold values from -0.125 to 0.125
- w_ffup: bfloat16 [2048, 2816], P('fs', 'tp'), may hold values from -0.125 to 0.125
- conv_gate: float32 [3, 2816], replicated, may hold values from -3 to 3
- conv_up: float32 [3, 2816], replicated, may hold values from -3 to 3
- w_down: bfloat16 [2816, 2048], P('tp', 'fs'), may hold values from -0.109375 to 0.109375
Outputs:
- layer_out: bfloat16 [16384, 2048], P(('rep', 'fs', 'tp')), parts along dimension 0
There are 2 independent parts, one for each index of `rep`. A program takes and returns all parts, laid end to end along the dimension named above; an argument that names none is the same for every part. Nothing has to cross between parts.
All inputs are finite; a program needn't handle non-finite values.
Results may differ from a plain program's by a relative error of at most 0.014.
Values may be sent and summed in bfloat16 or wider, within the bound.
A program may use at most 128 MiB of HBM per device.

v0:
```python
import jax
import jax.numpy as jnp
from jax import lax
from jax.sharding import PartitionSpec as P

HEADS = 4
DK = 128
DV = 256
KERNEL = 3
BLOCK = 128
LENGTH = 1024


epsilon = 1e-06


def rms_rows(matrix, scale_vec):
    values = matrix.astype(jnp.float32)
    factor = lax.rsqrt(jnp.mean(values * values, axis=-1, keepdims=True) + epsilon)
    return (values * factor * scale_vec).astype(jnp.bfloat16)


def rotate_heads(matrix):
    length = matrix.shape[0]
    half_width = matrix.shape[-1] // 2
    inverse = 10000.0 ** (-jnp.arange(half_width, dtype=jnp.float32) * 2.0 / (2 * half_width))
    angles = jnp.arange(length, dtype=jnp.float32)[:, None] * inverse[None, :]
    cosine = jnp.cos(angles)[:, None, :]
    sine = jnp.sin(angles)[:, None, :]
    values = matrix.astype(jnp.float32)
    first_half = values[..., :half_width]
    second_half = values[..., half_width:]
    return jnp.concatenate(
        [first_half * cosine - second_half * sine, first_half * sine + second_half * cosine],
        axis=-1,
    )


def retain_blocks(rot_query, rot_key, value, rates, block_len):
    length, head_count, width_k = rot_query.shape
    width_v = value.shape[-1]
    blocks = length // block_len
    query4 = rot_query.reshape(blocks, block_len, head_count, width_k)
    key4 = rot_key.reshape(blocks, block_len, head_count, width_k)
    value4 = value.reshape(blocks, block_len, head_count, width_v)
    places = jnp.arange(block_len, dtype=jnp.float32)
    spacing = places[:, None] - places[None, :]
    inside = jnp.where(
        spacing[None] >= 0, jnp.exp(-jnp.maximum(spacing, 0.0)[None] * rates[:, None, None]), 0.0
    )
    scores = jnp.einsum("cihd,cjhd->chij", query4, key4, preferred_element_type=jnp.float32)
    weights = (scores * inside[None]).astype(jnp.bfloat16)
    inner_part = jnp.einsum("chij,cjhe->cihe", weights, value4, preferred_element_type=jnp.float32)
    tail_decay = jnp.exp(-(block_len - 1.0 - places)[:, None] * rates[None, :])
    decayed = (key4.astype(jnp.float32) * tail_decay[None, :, :, None]).astype(jnp.bfloat16)
    states = jnp.einsum("cjhd,cjhe->chde", decayed, value4, preferred_element_type=jnp.float32)
    passing = jnp.exp(-block_len * rates)[:, None, None]

    def advance(carried, fresh):
        return (carried * passing + fresh, carried)

    _, before = lax.scan(advance, jnp.zeros((head_count, width_k, width_v), jnp.float32), states)
    onset_decay = jnp.exp(-(places + 1.0)[:, None] * rates[None, :])
    cross_part = (
        jnp.einsum(
            "cihd,chde->cihe", query4.astype(jnp.float32), before, precision=lax.Precision.HIGHEST
        )
        * onset_decay[None, :, :, None]
    )
    return (inner_part + cross_part).reshape(length, head_count, width_v)


def head_norm(retained):
    average = jnp.mean(retained, axis=-1, keepdims=True)
    centered = retained - average
    return centered * lax.rsqrt(jnp.mean(centered * centered, axis=-1, keepdims=True) + epsilon)


def causal_taps(matrix, kernel_w):
    length = matrix.shape[0]
    padded = jnp.pad(matrix.astype(jnp.float32), ((KERNEL - 1, 0), (0, 0)))
    total = jnp.zeros((length, matrix.shape[1]), jnp.float32)
    for tap_idx in range(KERNEL):
        total = total + kernel_w[tap_idx][None, :] * padded[tap_idx : tap_idx + length]
    return total


def collect_ffn(w_ffgate, w_ffup):
    return (
        lax.all_gather(w_ffgate, "fs", axis=0, tiled=True),
        lax.all_gather(w_ffup, "fs", axis=0, tiled=True),
    )


def body(
    tokens,
    mix_gain,
    w_query,
    w_key,
    w_value,
    w_out,
    ffn_gain,
    w_ffgate,
    w_ffup,
    conv_gate,
    conv_up,
    w_down,
):
    tp_rank = lax.axis_index("tp")
    heads_here = w_query.shape[1] // DK
    ffn_pair = None
    normed = rms_rows(tokens, mix_gain)
    query_w, key_w, value_w = (
        lax.all_gather(w_query, "fs", axis=0, tiled=True),
        lax.all_gather(w_key, "fs", axis=0, tiled=True),
        lax.all_gather(w_value, "fs", axis=0, tiled=True),
    )
    qk_cols = query_w.shape[1]
    pieces = lax.all_gather(normed, "tp", axis=0, tiled=True)
    joined = jnp.concatenate(
        [
            jnp.dot(pieces, query_w, preferred_element_type=jnp.float32),
            jnp.dot(pieces, key_w, preferred_element_type=jnp.float32),
            jnp.dot(pieces, value_w, preferred_element_type=jnp.float32),
        ],
        axis=1,
    ).astype(jnp.bfloat16)
    length = joined.shape[0]
    query = joined[:, :qk_cols].reshape(length, heads_here, DK)
    key = joined[:, qk_cols : 2 * qk_cols].reshape(length, heads_here, DK)
    value = joined[:, 2 * qk_cols :].reshape(length, heads_here, DV)
    rot_query = rotate_heads(query).astype(jnp.bfloat16)
    rot_key = (rotate_heads(key) * DK ** (-0.5)).astype(jnp.bfloat16)
    head_ids = (tp_rank * heads_here + jnp.arange(heads_here, dtype=jnp.int32)).astype(jnp.float32)
    rates = 1.0 / 16.0 * (32.0 / LENGTH) ** (head_ids / (HEADS - 1))
    retained = retain_blocks(rot_query, rot_key, value, rates, BLOCK)
    hidden = head_norm(retained).reshape(length, heads_here * DV).astype(jnp.bfloat16)
    out_full = lax.all_gather(w_out, "fs", axis=1, tiled=True)
    mix_sum = lax.psum_scatter(
        jnp.dot(hidden, out_full, preferred_element_type=jnp.float32).astype(jnp.bfloat16),
        "tp",
        scatter_dimension=0,
        tiled=True,
    ).astype(jnp.float32)
    resid = (tokens.astype(jnp.float32) + mix_sum).astype(jnp.bfloat16)
    normed_ffn = rms_rows(resid, ffn_gain)
    ff_here = w_ffgate.shape[1]
    ffn_pair = collect_ffn(w_ffgate, w_ffup)
    gate_w, up_w = ffn_pair
    pieces = lax.all_gather(normed_ffn, "tp", axis=0, tiled=True)
    both_pre = jnp.concatenate(
        [
            jnp.dot(pieces, gate_w, preferred_element_type=jnp.float32),
            jnp.dot(pieces, up_w, preferred_element_type=jnp.float32),
        ],
        axis=1,
    ).astype(jnp.bfloat16)
    gate_pre = both_pre[:, :ff_here]
    up_pre = both_pre[:, ff_here:]
    gate_taps = lax.dynamic_slice_in_dim(conv_gate, tp_rank * ff_here, ff_here, 1)
    up_taps = lax.dynamic_slice_in_dim(conv_up, tp_rank * ff_here, ff_here, 1)
    activ = (jax.nn.silu(causal_taps(gate_pre, gate_taps)) * causal_taps(up_pre, up_taps)).astype(
        jnp.bfloat16
    )
    down_full = lax.all_gather(w_down, "fs", axis=1, tiled=True)
    ffn_sum = lax.psum_scatter(
        jnp.dot(activ, down_full, preferred_element_type=jnp.float32).astype(jnp.bfloat16),
        "tp",
        scatter_dimension=0,
        tiled=True,
    ).astype(jnp.float32)
    return (resid.astype(jnp.float32) + ffn_sum).astype(jnp.bfloat16)


def solution(mesh):
    placed = (
        P(("rep", "fs", "tp"), None),
        P(),
        P("fs", "tp"),
        P("fs", "tp"),
        P("fs", "tp"),
        P("tp", "fs"),
        P(),
        P("fs", "tp"),
        P("fs", "tp"),
        P(),
        P(),
        P("tp", "fs"),
    )
    return jax.shard_map(
        body, mesh=mesh, in_specs=placed, out_specs=P(("rep", "fs", "tp"), None), check_vma=False
    )
```

profile of v0, /device:TPU:0, one launch (start us, length us, event | category | flops | bytes accessed | tf_op | source)
XLA Modules:
  0.0 569.6 jit_solution(2240362680662061393)
XLA Ops:
  6.5 0.7 all-gather.14.cloned.1.call-update
  7.3 2.1 fusion.2
  9.4 3.5 fusion.4
  13.0 0.7 all-gather.16.cloned.1.call-update
  14.3 0.5 all-gather.18.cloned.1.call-update
  15.0 1.0 fusion.23
  16.2 36.3 %all-gather.14.cloned.1.call-done = bf16[2048,256]{1,0:T(8,128)(2,1)} async-done(((bf16[256,256]{1,0:T(8,128)(2,1)}), bf16[2048,256]{1,0:T(8,128)(2,1)}) %all-gather.14.cloned.1.call-update) | async-done | bytes 1048592 | tf_op jit(solution)/shard_map/all_gather | solution.py:114
  52.5 14.0 %all-gather.10.cloned.1.call-done = bf16[1024,2048]{1,0:T(8,128)(2,1)} async-done(((bf16[512,2048]{1,0:T(8,128)(2,1)}), bf16[1024,2048]{1,0:T(8,128)(2,1)}) %all-gather.10.cloned.1.call-update) | async-done | bytes 4194320 | tf_op jit(solution)/shard_map/all_gather | solution.py:119
  66.4 3.8 convolution_convert_fusion.6
  70.3 39.7 %all-gather.16.cloned.1.call-done = bf16[2048,256]{1,0:T(8,128)(2,1)} async-done(((bf16[256,256]{1,0:T(8,128)(2,1)}), bf16[2048,256]{1,0:T(8,128)(2,1)}) %all-gather.16.cloned.1.call-update) | async-done | bytes 1048592 | tf_op jit(solution)/shard_map/all_gather | solution.py:115
  110.1 3.8 convolution_convert_fusion.5
  114.0 1.1 subtract_convert_fusion
  116.0 43.8 %all-gather.12.cloned.1.call-done = bf16[2048,512]{1,0:T(8,128)(2,1)} async-done(((bf16[256,512]{1,0:T(8,128)(2,1)}), bf16[2048,512]{1,0:T(8,128)(2,1)}) %all-gather.12.cloned.1.call-update) | async-done | bytes 2097168 | tf_op jit(solution)/shard_map/all_gather | solution.py:116
  159.9 6.3 %convolution_convert_fusion.4 = bf16[1024,512]{1,0:T(8,128)(2,1)} fusion(bf16[1024,2048]{1,0:T(8,128)(2,1)} %all-gather.10.cloned.1.call-done, bf16[2048,512]{1,0:T(8,128)(2,1)} %all-gather.12.cloned.1.call-done), kind=kOutput, calls=%fused_computation.31 | convolution fusion | flops 2148007936 | bytes 7340032 | tf_op jit(solution)/shard_map/dot_general | solution.py:124
  166.1 1.4 reshape_reshape.3
  167.9 0.8 copy-done.4
  168.7 0.6 fusion.18
  169.2 6.9 %while.13 = (s32[]{:T(128)}, f32[2,128,256]{2,1,0:T(8,128)S(1)}, f32[8,2,128,256]{3,2,1,0:T(8,128)}, f32[8,2,128,256]{3,2,1,0:T(8,128)S(1)}, s32[]{:T(128)}, /*index=5*/s32[]{:T(128)}, s32[]{:T(128)}) while((s32[]{:T(128)}, f32[2,128,256]{2,1,0:T(8,128)S(1)}, f32[8,2,128,256]{3,2,1,0:T(8,128)}, f32[8,2,128,256]{3,2,1,0:T(8,128)S(1)}, ...), condition=%wide.region_2.3_spmd.clone, body=%wide.region_1.2_spmd.clone.sunk | while | flops 262155 | bytes 1311344 | solution.py:62
  169.2 0.7 bitcast_dynamic-update-slice_fusion.2
  170.1 0.7 bitcast_dynamic-update-slice_fusion.2
  171.0 0.7 bitcast_dynamic-update-slice_fusion.2
  171.8 0.7 bitcast_dynamic-update-slice_fusion.2
  172.7 0.7 bitcast_dynamic-update-slice_fusion.2
  173.6 0.7 bitcast_dynamic-update-slice_fusion.2
  174.4 0.7 bitcast_dynamic-update-slice_fusion.2
  175.3 0.7 bitcast_dynamic-update-slice_fusion.2
  176.1 1.0 copy.39
  177.5 1.2 copy.40
  179.0 5.2 fusion.24
  184.2 3.0 fusion.32
  187.3 1.2 copy.36
  189.3 21.6 %all-gather.18.cloned.1.call-done = bf16[512,2048]{1,0:T(8,128)(2,1)} async-done(((bf16[512,256]{1,0:T(8,128)(2,1)}), bf16[512,2048]{1,0:T(8,128)(2,1)}) %all-gather.18.cloned.1.call-update) | async-done | bytes 2097168 | tf_op jit(solution)/shard_map/all_gather | solution.py:138
  210.9 5.9 %convolution_convert_fusion.3 = bf16[1024,2048]{1,0:T(8,128)(2,1)} fusion(bf16[1024,512]{0,1:T(8,128)(2,1)S(1)} %fusion.13, bf16[512,2048]{1,0:T(8,128)(2,1)} %all-gather.18.cloned.1.call-done), kind=kOutput, calls=%fused_computation.24 | convolution fusion | flops 2149580800 | bytes 7340032 | tf_op jit(solution)/shard_map/dot_general | solution.py:140
  216.9 0.7 all-gather.24.cloned.1.call-update
  217.6 9.6 %reduce-scatter.3.cloned.1.call-done = bf16[512,2048]{1,0:T(8,128)(2,1)} async-done(((bf16[1024,2048]{1,0:T(8,128)(2,1)}), bf16[512,2048]{1,0:T(8,128)(2,1)}) %reduce-scatter.3.cloned.1.call-update) | async-done | bytes 2097168 | tf_op jit(solution)/shard_map/reduce_scatter | solution.py:139
  227.2 2.5 fusion.6
  229.7 2.4 fusion.8
  232.2 0.7 all-gather.22.cloned.1.call-update
  233.5 1.0 dynamic-slice_reduce_fusion.2
  234.5 88.5 %all-gather.24.cloned.1.call-done = bf16[2048,1408]{1,0:T(8,128)(2,1)} async-done(((bf16[256,1408]{1,0:T(8,128)(2,1)}), bf16[2048,1408]{1,0:T(8,128)(2,1)}) %all-gather.24.cloned.1.call-update) | async-done | bytes 5767184 | tf_op jit(solution)/shard_map/all_gather | solution.py:91
  323.0 13.4 %all-gather.20.cloned.1.call-done = bf16[1024,2048]{1,0:T(8,128)(2,1)} async-done(((bf16[512,2048]{1,0:T(8,128)(2,1)}), bf16[1024,2048]{1,0:T(8,128)(2,1)}) %all-gather.20.cloned.1.call-update) | async-done | bytes 4194320 | tf_op jit(solution)/shard_map/all_gather | solution.py:150
  336.4 11.7 %fusion.10 = f32[1024,1408]{1,0:T(8,128)} fusion(bf16[1024,2048]{1,0:T(8,128)(2,1)} %all-gather.20.cloned.1.call-done, bf16[2048,1408]{1,0:T(8,128)(2,1)} %all-gather.24.cloned.1.call-done), kind=kOutput, calls=%fused_computation.20 | convolution fusion | flops 5908463616 | bytes 15728640 | tf_op jit(solution)/shard_map/dot_general | solution.py:154
  348.1 84.0 %all-gather.22.cloned.1.call-done = bf16[2048,1408]{1,0:T(8,128)(2,1)} async-done(((bf16[256,1408]{1,0:T(8,128)(2,1)}), bf16[2048,1408]{1,0:T(8,128)(2,1)}) %all-gather.22.cloned.1.call-update) | async-done | bytes 5767184 | tf_op jit(solution)/shard_map/all_gather | solution.py:90
  432.1 11.7 %fusion.11 = f32[1024,1408]{1,0:T(8,128)} fusion(bf16[1024,2048]{1,0:T(8,128)(2,1)} %all-gather.20.cloned.1.call-done, bf16[2048,1408]{1,0:T(8,128)(2,1)} %all-gather.22.cloned.1.call-done), kind=kOutput, calls=%fused_computation.22 | convolution fusion | flops 5908463616 | bytes 15728640 | tf_op jit(solution)/shard_map/dot_general | solution.py:153
  443.8 81.5 %all-gather.26.cloned.1.call-done = bf16[1408,2048]{1,0:T(8,128)(2,1)} async-done(((bf16[1408,256]{1,0:T(8,128)(2,1)}), bf16[1408,2048]{1,0:T(8,128)(2,1)}) %all-gather.26.cloned.1.call-update) | async-done | bytes 5767184 | tf_op jit(solution)/shard_map/all_gather | solution.py:165
  525.4 22.6 %convolution_convert_fusion.2 = bf16[1024,2048]{1,0:T(8,128)(2,1)} fusion(bf16[1408,2048]{1,0:T(8,128)(2,1)} %all-gather.26.cloned.1.call-done, f32[1024,1408]{1,0:T(8,128)} %fusion.10, f32[1024,1408]{1,0:T(8,128)} %fusion.11, f32[1408]{0:T(1024)S(1)} %get-tuple-element.59, f32[1408]{0:T(1024)S(1)} %get-tuple-element.58, f32[1408]{0:T(1024)S(1)} %get-tuple-element.57, ...), kind=kOutput, calls=%fused_computation.23 | convolution fusion | flops 5930745856 | bytes 21529600 | tf_op jit(solution)/shard_map/dot_general | solution.py:167
  548.0 10.4 %reduce-scatter.5.cloned.1.call-done = bf16[512,2048]{1,0:T(8,128)(2,1)} async-done(((bf16[1024,2048]{1,0:T(8,128)(2,1)}), bf16[512,2048]{1,0:T(8,128)(2,1)}) %reduce-scatter.5.cloned.1.call-update) | async-done | bytes 2097168 | tf_op jit(solution)/shard_map/reduce_scatter | solution.py:166
  558.3 4.8 fusion.9
  (68 shorter events, 5.6 us)
Async XLA Ops:
  6.5 46.0 %all-gather.14.cloned.1.call-start = ((), (), s32[]{:S(2)}) async-start(), calls=%async_computation.4 | async-start | bytes 1179648 | tf_op jit(solution)/shard_map/all_gather | solution.py:114
  7.3 59.2 %all-gather.10.cloned.1.call-start = ((), (), s32[]{:S(2)}) async-start(), calls=%async_computation.2 | async-start | bytes 6291456 | tf_op jit(solution)/shard_map/all_gather | solution.py:119
  12.9 97.1 %all-gather.16.cloned.1.call-start = ((), (), s32[]{:S(2)}) async-start(), calls=%async_computation.5 | async-start | bytes 1179648 | tf_op jit(solution)/shard_map/all_gather | solution.py:115
  13.7 146.2 %all-gather.12.cloned.1.call-start = ((), (), s32[]{:S(2)}) async-start(), calls=%async_computation.3 | async-start | bytes 2359296 | tf_op jit(solution)/shard_map/all_gather | solution.py:116
  14.2 196.6 %all-gather.18.cloned.1.call-start = ((), (), s32[]{:S(2)}) async-start(), calls=%async_computation.6 | async-start | bytes 2359296 | tf_op jit(solution)/shard_map/all_gather | solution.py:138
  14.8 212.4 %reduce-scatter.3.cloned.1.call-start = ((), (), s32[]{:S(2)}) async-start(), calls=%async_computation.7 | async-start | bytes 6291456 | tf_op jit(solution)/shard_map/reduce_scatter | solution.py:139
  167.9 0.8 copy-start.4
  177.5 6.8 %copy-start.2 = (bf16[8,128,2,64]{3,1,2,0:T(8,128)(2,1)}, bf16[8,128,2,64]{3,1,2,0:T(8,128)(2,1)S(1)}, u32[]{:S(2)}) copy-start(bf16[8,128,2,64]{3,1,2,0:T(8,128)(2,1)S(1)} %copy.28) | copy-start | bytes 786436
  179.0 5.3 copy-start.3
  216.8 10.4 %copy-start = (bf16[512,2048]{1,0:T(8,128)(2,1)S(1)}, bf16[512,2048]{1,0:T(8,128)(2,1)}, u32[]{:S(2)}) copy-start(bf16[512,2048]{1,0:T(8,128)(2,1)} %param.14) | copy-start | bytes 6291460
  216.8 12.9 %copy-start.5 = (f32[2048]{0:T(1024)S(1)}, f32[2048]{0:T(1024)}, u32[]{:S(2)}) copy-start(f32[2048]{0:T(1024)} %param.20) | copy-start | bytes 24580
  216.8 106.2 %all-gather.24.cloned.1.call-start = ((), (), s32[]{:S(2)}) async-start(), calls=%async_computation.10 | async-start | bytes 6488064 | tf_op jit(solution)/shard_map/all_gather | solution.py:91
  217.6 118.8 %all-gather.20.cloned.1.call-start = ((), (), s32[]{:S(2)}) async-start(), calls=%async_computation.8 | async-start | bytes 6291456 | tf_op jit(solution)/shard_map/all_gather | solution.py:150
  227.2 2.5 copy-start.1
  232.1 200.0 %all-gather.22.cloned.1.call-start = ((), (), s32[]{:S(2)}) async-start(), calls=%async_computation.9 | async-start | bytes 6488064 | tf_op jit(solution)/shard_map/all_gather | solution.py:90
  232.8 292.5 %all-gather.26.cloned.1.call-start = ((), (), s32[]{:S(2)}) async-start(), calls=%async_computation.11 | async-start | bytes 6488064 | tf_op jit(solution)/shard_map/all_gather | solution.py:165
  233.4 324.9 %reduce-scatter.5.cloned.1.call-start = ((), (), s32[]{:S(2)}) async-start(), calls=%async_computation.12 | async-start | bytes 6291456 | tf_op jit(solution)/shard_map/reduce_scatter | solution.py:166
Sparse Core Ops, SparseCore 0:
  9.5 42.9 all-gather.13
  54.0 12.3 all-gather.9
  68.6 41.4 all-gather.15
  112.0 47.7 all-gather.11
  161.8 49.0 all-gather.17
  216.9 10.2 reduce-scatter.2
  229.4 93.5 all-gather.23
  324.5 11.8 all-gather.19
  338.6 93.4 all-gather.21
  434.0 91.3 all-gather.25
  548.1 10.1 reduce-scatter.4
where the time goes:
time: 570 us
  waiting for transfers between devices  447 us (78%)
  matrix products  74.6 us (13%)
  other arithmetic  25.6 us (4%)
  between operations  13.5 us (2%)
  local copies, waits for them, and re-layouts  8.11 us (1%)
    all_gather x1, waiting for transfers between devices, collect_ffn(): lax.all_gather(w_ffup, 'fs', axis=0, tiled=True)  88.5 us
    all_gather x1, waiting for transfers between devices, collect_ffn(): lax.all_gather(w_ffgate, 'fs', axis=0, tiled=True)  84 us
    all_gather x1, waiting for transfers between devices, body(): down_full = lax.all_gather(w_down, 'fs', axis=1, tiled=True)  81.5 us
    all_gather x1, waiting for transfers between devices, body(): lax.all_gather(w_value, 'fs', axis=0, tiled=True)  43.8 us
    all_gather x1, waiting for transfers between devices, body(): lax.all_gather(w_key, 'fs', axis=0, tiled=True)  39.7 us
    all_gather x1, waiting for transfers between devices, body(): lax.all_gather(w_query, 'fs', axis=0, tiled=True)  36.3 us
    dot_general x1, matrix products, body(): jnp.dot(activ, down_full, preferred_element_type=jnp.float32)  22.6 us
    all_gather x1, waiting for transfers between devices, body(): out_full = lax.all_gather(w_out, 'fs', axis=1, tiled=True)  21.6 us
  transfers between devices with their start and end apart: 11, of which 11 were waited for; matrix products, arithmetic and copies ran while one was open for 13% of the time, Pallas kernels for 0%

commit v1 on v0

--- a/solution.py
+++ b/solution.py
@@ -1,6 +1,10 @@
+import functools
+
 import jax
 import jax.numpy as jnp
 from jax import lax
+from jax.experimental import pallas as pl
+from jax.experimental.pallas import tpu as pltpu
 from jax.sharding import PartitionSpec as P
 
 HEADS = 4
@@ -9,9 +13,230 @@
 KERNEL = 3
 BLOCK = 128
 LENGTH = 1024
+MESH = pl.DeviceIdType.MESH
+ROWS, COLS = "rows", "cols"
 
 
 epsilon = 1e-06
+
+
+def gather_kernel(sizes, kinds, *refs):
+    reps, fs, tps = sizes
+    count = len(kinds)
+    tokens = refs[0]
+    shards = refs[1 : 1 + count]
+    both = refs[1 + count]
+    fulls = refs[2 + count : 2 + 2 * count]
+    (tok_sems, own_sems, up_send, up_recv, down_send, down_recv, y_send, y_recv, x_send, x_recv) = refs[
+        2 + 2 * count :
+    ]
+    depth = fs // 2
+    rep = lax.axis_index("rep")
+    place = lax.axis_index("fs")
+    core = lax.axis_index("tp")
+    z = place // 2
+    y = lax.rem(place, 2)
+    above = {"fs": lax.rem(place + 2, fs)}
+    below = {"fs": lax.rem(place + fs - 2, fs)}
+    beside = {"fs": z * 2 + 1 - y}
+    twin = {"rep": 1 - rep}
+    other = {"tp": 1 - core}
+
+    barrier = pltpu.get_barrier_semaphore()
+
+    def greet(device):
+        pl.semaphore_signal(barrier, inc=1, device_id=device, device_id_type=MESH)
+
+    greet(beside)
+    greet(twin)
+    greet(other)
+    pl.when(z < depth - 1)(lambda: greet(above))
+    pl.when(z > 0)(lambda: greet(below))
+    at_end = (z == 0) | (z == depth - 1)
+    pl.when(at_end)(lambda: pl.semaphore_wait(barrier, 4))
+    pl.when(jnp.logical_not(at_end))(lambda: pl.semaphore_wait(barrier, 5))
+
+    def slot(p, owner, start, size):
+        rows, cols = shards[p].shape
+        start = pl.multiple_of(start, 16)
+        if kinds[p] == COLS:
+            return fulls[p].at[pl.ds(start, size), pl.ds(pl.multiple_of(owner * cols, 128), cols)]
+        return fulls[p].at[pl.ds(pl.multiple_of(owner * rows, 16) + start, size)]
+
+    def spans(p):
+        rows = shards[p].shape[0]
+        third = rows * 5 // 16 // 16 * 16
+        return third, rows - third
+
+    def piece(p, owner, own):
+        third, most = spans(p)
+        start = rep * third
+        src = shards[p].at[pl.ds(pl.multiple_of(start, 16), most)] if own else slot(p, owner, start, most)
+        return src, slot(p, owner, start, most)
+
+    def copy(src, dst, send, recv, device):
+        return pltpu.make_async_remote_copy(
+            src_ref=src, dst_ref=dst, send_sem=send, recv_sem=recv, device_id=device, device_id_type=MESH
+        )
+
+    def clip(value):
+        return jnp.minimum(jnp.maximum(value, 0), depth - 1)
+
+    def up(p, s):
+        src, dst = piece(p, clip(z - s) * 2 + y, s == 0)
+        return copy(src, dst, up_send.at[p, s], up_recv.at[p, s], above)
+
+    def down(p, s):
+        src, dst = piece(p, clip(z + s) * 2 + y, s == 0)
+        return copy(src, dst, down_send.at[p, s], down_recv.at[p, s], below)
+
+    def up_in(p, s):
+        dst = piece(p, clip(z - 1 - s) * 2 + y, False)[1]
+        return copy(dst, dst, up_send.at[p, s], up_recv.at[p, s], above)
+
+    def down_in(p, s):
+        dst = piece(p, clip(z + 1 + s) * 2 + y, False)[1]
+        return copy(dst, dst, down_send.at[p, s], down_recv.at[p, s], below)
+
+    def level(k):
+        return z if k == 0 else (clip(z - k) if k < depth else clip(z + k - depth + 1))
+
+    def valid(k):
+        return z >= 0 if k == 0 else (z - k >= 0 if k < depth else z + k - depth + 1 < depth)
+
+    def y_copy(p, k):
+        src, dst = piece(p, level(k) * 2 + y, k == 0)
+        return copy(src, dst, y_send.at[p, k], y_recv.at[p, k], beside)
+
+    def y_in(p, k):
+        dst = piece(p, level(k) * 2 + 1 - y, False)[1]
+        return copy(dst, dst, y_send.at[p, k], y_recv.at[p, k], beside)
+
+    kmax = 2 * depth - 1
+
+    def x_copy(p, k, side, mine):
+        third, most = spans(p)
+        who = rep if mine else 1 - rep
+        lane = y if side == 0 else 1 - y
+        ref = slot(p, level(k) * 2 + lane, who * most, third)
+        return copy(ref, ref, x_send.at[p, side * kmax + k], x_recv.at[p, side * kmax + k], twin)
+
+    tok_rows = tokens.shape[0]
+    here = both.at[pl.ds(pl.multiple_of(core * tok_rows, 16), tok_rows)]
+    tok_out = copy(tokens, here, tok_sems.at[0], tok_sems.at[1], other)
+    tok_out.start()
+    tok_own = pltpu.make_async_copy(tokens, here, tok_sems.at[2])
+    tok_own.start()
+    owns = []
+    for p in range(count):
+        own = pltpu.make_async_copy(shards[p], slot(p, place, 0, shards[p].shape[0]), own_sems.at[p])
+        own.start()
+        owns.append(own)
+
+    steps = depth - 1
+    events = [(p, s) for p in range(count) for s in range(steps)]
+
+    def start_z(p, s):
+        pl.when((z - s >= 0) & (z < depth - 1))(lambda: up(p, s).start())
+        pl.when((z + s <= depth - 1) & (z > 0))(lambda: down(p, s).start())
+        if s == 0:
+            y_copy(p, 0).start()
+
+    def take_z(p, s):
+        ku, kd = s + 1, depth + s
+
+        @pl.when(z - 1 - s >= 0)
+        def _():
+            up_in(p, s).wait_recv()
+
+        @pl.when(z + 1 + s <= depth - 1)
+        def _():
+            down_in(p, s).wait_recv()
+
+    def spread(p, s):
+        for k in (s + 1, depth + s):
+
+            @pl.when(valid(k))
+            def _():
+                y_copy(p, k).start()
+                x_copy(p, k, 0, True).start()
+
+    def take_y(p, k):
+        @pl.when(valid(k))
+        def _():
+            y_in(p, k).wait_recv()
+            x_copy(p, k, 1, True).start()
+
+    def finish_y(p, s):
+        if s == 0:
+            take_y(p, 0)
+        take_y(p, s + 1)
+        take_y(p, depth + s)
+
+    lag = 2
+    total = len(events)
+    start_z(*events[0])
+    for e in range(total + lag):
+        if e < total:
+            take_z(*events[e])
+            if e + 1 < total:
+                start_z(*events[e + 1])
+            spread(*events[e])
+        if e >= lag:
+            finish_y(*events[e - lag])
+
+    for p in range(count):
+        for k in range(kmax):
+
+            @pl.when(valid(k))
+            def _():
+                if k > 0:
+                    x_copy(p, k, 0, False).wait_recv()
+                    x_copy(p, k, 0, True).wait_send()
+                x_copy(p, k, 1, False).wait_recv()
+                x_copy(p, k, 1, True).wait_send()
+                y_copy(p, k).wait_send()
+
+        for s in range(steps):
+            pl.when((z - s >= 0) & (z < depth - 1))(lambda: up(p, s).wait_send())
+            pl.when((z + s <= depth - 1) & (z > 0))(lambda: down(p, s).wait_send())
+    for own in owns:
+        own.wait()
+    tok_own.wait()
+    tok_out.wait()
+
+
+def gather_all(sizes, tokens, shards):
+    fs = sizes[1]
+    kinds = []
+    outs = [jax.ShapeDtypeStruct((tokens.shape[0] * 2, tokens.shape[1]), tokens.dtype)]
+    for shard, by_cols in shards:
+        rows, cols = shard.shape
+        side = by_cols and cols % 128 == 0
+        kinds.append(COLS if side else ROWS)
+        outs.append(jax.ShapeDtypeStruct((rows, cols * fs) if side else (rows * fs, cols), shard.dtype))
+    count, depth = len(shards), fs // 2
+    dma = pltpu.SemaphoreType.DMA
+    vmem = pl.BlockSpec(memory_space=pltpu.VMEM)
+    anywhere = pl.BlockSpec(memory_space=pl.ANY)
+    got = pl.pallas_call(
+        functools.partial(gather_kernel, sizes, tuple(kinds)),
+        out_shape=outs,
+        in_specs=[vmem] * (count + 1),
+        out_specs=[anywhere] * (count + 1),
+        scratch_shapes=[dma((3,)), dma((count,))]
+        + [dma((count, depth - 1))] * 4
+        + [dma((count, 2 * depth - 1))] * 2
+        + [dma((count, 4 * depth - 2))] * 2,
+        compiler_params=pltpu.CompilerParams(collective_id=0, has_side_effects=True),
+    )(tokens, *[shard for shard, _ in shards])
+    fulls = []
+    for full, (shard, by_cols), kind in zip(got[1:], shards, kinds):
+        if by_cols and kind == ROWS:
+            rows, cols = shard.shape
+            full = full.reshape(fs, rows, cols).transpose(1, 0, 2).reshape(rows, fs * cols)
+        fulls.append(full)
+    return got[0], fulls
 
 
 def rms_rows(matrix, scale_vec):
@@ -85,14 +310,22 @@
     return total
 
 
-def collect_ffn(w_ffgate, w_ffup):
-    return (
-        lax.all_gather(w_ffgate, "fs", axis=0, tiled=True),
-        lax.all_gather(w_ffup, "fs", axis=0, tiled=True),
-    )
+def sum_over_tp(partial, tp_rank):
+    rows = partial.shape[0] // 2
+    mine = lax.dynamic_slice_in_dim(partial, tp_rank * rows, rows, 0)
+    theirs = lax.dynamic_slice_in_dim(partial, (1 - tp_rank) * rows, rows, 0)
+    got = lax.ppermute(theirs, "tp", [(0, 1), (1, 0)])
+    return mine.astype(jnp.float32) + got.astype(jnp.float32)
+
+
+def share_over_tp(matrix, tp_rank):
+    got = lax.ppermute(matrix, "tp", [(0, 1), (1, 0)])
+    first = tp_rank == 0
+    return jnp.concatenate([jnp.where(first, matrix, got), jnp.where(first, got, matrix)], axis=0)
 
 
 def body(
+    sizes,
     tokens,
     mix_gain,
     w_query,
@@ -108,23 +341,15 @@
 ):
     tp_rank = lax.axis_index("tp")
     heads_here = w_query.shape[1] // DK
-    ffn_pair = None
-    normed = rms_rows(tokens, mix_gain)
-    query_w, key_w, value_w = (
-        lax.all_gather(w_query, "fs", axis=0, tiled=True),
-        lax.all_gather(w_key, "fs", axis=0, tiled=True),
-        lax.all_gather(w_value, "fs", axis=0, tiled=True),
-    )
-    qk_cols = query_w.shape[1]
-    pieces = lax.all_gather(normed, "tp", axis=0, tiled=True)
-    joined = jnp.concatenate(
-        [
-            jnp.dot(pieces, query_w, preferred_element_type=jnp.float32),
-            jnp.dot(pieces, key_w, preferred_element_type=jnp.float32),
-            jnp.dot(pieces, value_w, preferred_element_type=jnp.float32),
-        ],
-        axis=1,
-    ).astype(jnp.bfloat16)
+    qk_cols = w_query.shape[1]
+    qkv_shard = jnp.concatenate([w_query, w_key, w_value], axis=1)
+    both, (qkv_w, out_full, gate_w, up_w, down_full) = gather_all(
+        sizes,
+        tokens,
+        ((qkv_shard, False), (w_out, True), (w_ffgate, False), (w_ffup, False), (w_down, True)),
+    )
+    pieces = rms_rows(both, mix_gain)
+    joined = jnp.dot(pieces, qkv_w, preferred_element_type=jnp.float32).astype(jnp.bfloat16)
     length = joined.shape[0]
     query = joined[:, :qk_cols].reshape(length, heads_here, DK)
     key = joined[:, qk_cols : 2 * qk_cols].reshape(length, heads_here, DK)
@@ -135,44 +360,28 @@
     rates = 1.0 / 16.0 * (32.0 / LENGTH) ** (head_ids / (HEADS - 1))
     retained = retain_blocks(rot_query, rot_key, value, rates, BLOCK)
     hidden = head_norm(retained).reshape(length, heads_here * DV).astype(jnp.bfloat16)
-    out_full = lax.all_gather(w_out, "fs", axis=1, tiled=True)
-    mix_sum = lax.psum_scatter(
-        jnp.dot(hidden, out_full, preferred_element_type=jnp.float32).astype(jnp.bfloat16),
-        "tp",
-        scatter_dimension=0,
-        tiled=True,
-    ).astype(jnp.float32)
+    mix_sum = sum_over_tp(
+        jnp.dot(hidden, out_full, preferred_element_type=jnp.float32).astype(jnp.bfloat16), tp_rank
+    )
     resid = (tokens.astype(jnp.float32) + mix_sum).astype(jnp.bfloat16)
     normed_ffn = rms_rows(resid, ffn_gain)
     ff_here = w_ffgate.shape[1]
-    ffn_pair = collect_ffn(w_ffgate, w_ffup)
-    gate_w, up_w = ffn_pair
-    pieces = lax.all_gather(normed_ffn, "tp", axis=0, tiled=True)
-    both_pre = jnp.concatenate(
-        [
-            jnp.dot(pieces, gate_w, preferred_element_type=jnp.float32),
-            jnp.dot(pieces, up_w, preferred_element_type=jnp.float32),
-        ],
-        axis=1,
-    ).astype(jnp.bfloat16)
-    gate_pre = both_pre[:, :ff_here]
-    up_pre = both_pre[:, ff_here:]
+    pieces = share_over_tp(normed_ffn, tp_rank)
+    gate_pre = jnp.dot(pieces, gate_w, preferred_element_type=jnp.float32).astype(jnp.bfloat16)
+    up_pre = jnp.dot(pieces, up_w, preferred_element_type=jnp.float32).astype(jnp.bfloat16)
     gate_taps = lax.dynamic_slice_in_dim(conv_gate, tp_rank * ff_here, ff_here, 1)
     up_taps = lax.dynamic_slice_in_dim(conv_up, tp_rank * ff_here, ff_here, 1)
     activ = (jax.nn.silu(causal_taps(gate_pre, gate_taps)) * causal_taps(up_pre, up_taps)).astype(
         jnp.bfloat16
     )
-    down_full = lax.all_gather(w_down, "fs", axis=1, tiled=True)
-    ffn_sum = lax.psum_scatter(
-        jnp.dot(activ, down_full, preferred_element_type=jnp.float32).astype(jnp.bfloat16),
-        "tp",
-        scatter_dimension=0,
-        tiled=True,
-    ).astype(jnp.float32)
+    ffn_sum = sum_over_tp(
+        jnp.dot(activ, down_full, preferred_element_type=jnp.float32).astype(jnp.bfloat16), tp_rank
+    )
     return (resid.astype(jnp.float32) + ffn_sum).astype(jnp.bfloat16)
 
 
 def solution(mesh):
+    sizes = (mesh.shape["rep"], mesh.shape["fs"], mesh.shape["tp"])
     placed = (
         P(("rep", "fs", "tp"), None),
         P(),
@@ -188,5 +397,6 @@
         P("tp", "fs"),
     )
     return jax.shard_map(
-        body, mesh=mesh, in_specs=placed, out_specs=P(("rep", "fs", "tp"), None), check_vma=False
-    )
+        functools.partial(body, sizes),
+        mesh=mesh, in_specs=placed, out_specs=P(("rep", "fs", "tp"), None), check_vma=False
+    )

time: 570 us -> 318 us (0.56)
  waiting for transfers between devices: 447 us -> 11.7 us
  Pallas kernels: 0 us -> 194 us
  between operations: 13.5 us -> 0.33 us
  matrix products: 74.6 us -> 65.1 us
  local copies, waits for them, and re-layouts: 8.11 us -> 16.7 us
    all_gather x9 -> x0, waiting for transfers between devices: 423 us -> none  [the longest x1 88.5 us: collect_ffn(): lax.all_gather(w_ffup, 'fs', axis=0, tiled=True)]
    pallas_call x0 -> x1, Pallas kernels: none -> 194 us  [gather_all(): pl.pallas_call(functools.partial(gather_kernel, sizes, tuple(kinds)), out...]
    reduce_scatter x2 -> x0, waiting for transfers between devices: 19.9 us -> none  [the longest x1 10.4 us: body(): lax.psum_scatter(jnp.dot(activ, down_full, preferred_element_type=jnp.flo...]
    ppermute x0 -> x3, waiting for transfers between devices: none -> 11.7 us  [the longest x2 8.29 us: sum_over_tp(): got = lax.ppermute(theirs, 'tp', [(0, 1), (1, 0)])]
    dot_general x3 -> x1, matrix products: 13.8 us -> 7.45 us  [body(): jnp.dot(pieces, qkv_w, preferred_element_type=jnp.float32)]
  transfers between devices with their start and end apart: 11 -> 3, of which waited for: 11 -> 3; matrix products, arithmetic and copies ran while one was open for 13% -> 0% of each run, Pallas kernels for 0% -> 0%
where the time goes in v1:
time: 318 us; the launch traced here: 317 us
  Pallas kernels  194 us (61%)
  matrix products  65.1 us (20%)
  other arithmetic  28.9 us (9%)
  local copies, waits for them, and re-layouts  16.7 us (5%)
  waiting for transfers between devices  11.7 us (4%)
    pallas_call x1, Pallas kernels, gather_all(): pl.pallas_call(functools.partial(gather_kernel, sizes, tuple(kinds)), out...  194 us
    dot_general x1, matrix products, body(): jnp.dot(activ, down_full, preferred_element_type=jnp.float32)  22.7 us
    dot_general x1, matrix products, body(): jnp.dot(pieces, gate_w, preferred_element_type=jnp.float32)  10.7 us
    dot_general x1, matrix products, body(): jnp.dot(pieces, up_w, preferred_element_type=jnp.float32)  9.63 us
    ppermute x2, waiting for transfers between devices, sum_over_tp(): got = lax.ppermute(theirs, 'tp', [(0, 1), (1, 0)])  8.29 us
    dot_general x1, matrix products, body(): jnp.dot(pieces, qkv_w, preferred_element_type=jnp.float32)  7.45 us
    reduce_sum x2, other arithmetic, rms_rows(): jnp.mean(values * values, axis=-1, keepdims=True) + epsilon  7.34 us
  transfers between devices with their start and end apart: 3, of which 3 were waited for; matrix products, arithmetic and copies ran while one was open for 0% of the time, Pallas kernels for 0%

profile of v1, /device:TPU:0, one launch (start us, length us, event | category | flops | bytes accessed | tf_op | source)
XLA Modules:
  0.0 317.2 jit_solution(14859516821899811392)
XLA Ops:
  0.0 1.9 pad_maximum_fusion.3.refs_1_
  1.9 193.7 %shard_map.118 = (bf16[1024,2048]{1,0:T(8,128)(2,1)}, bf16[2048,1024]{1,0:T(8,128)(2,1)}, bf16[512,2048]{1,0:T(8,128)(2,1)}, bf16[2048,1408]{1,0:T(8,128)(2,1)},...) custom-call(bf16[512,2048]{1,0:T(8,128)(2,1)} %refs_0_.1, bf16[256,1024]{1,0:T(8,128)(2,1)} %pad_maximum_fusion.3.refs_1_, ...), custom_call_target="tpu_custom_call" | custom-call | tf_op jit(solution)/shard_map/pallas_call | solution.py:222
  195.6 3.2 %fusion.2 = f32[1024]{0:T(1024)S(1)} fusion(bf16[1024,2048]{1,0:T(8,128)(2,1)} %get-tuple-element.38), kind=kLoop, calls=%fused_computation.6 | loop fusion | flops 6290432 | bytes 4198400 | tf_op jit(solution)/shard_map/reduce_sum | solution.py:244
  198.9 0.2 copy-done.3
  199.1 7.5 %fusion.18 = bf16[1024,1024]{0,1:T(8,128)(2,1)S(1)} fusion(bf16[2048,1024]{1,0:T(8,128)(2,1)} %get-tuple-element.39, bf16[1024,2048]{1,0:T(8,128)(2,1)S(1)} %copy-done.3, f32[2048]{0:T(1024)S(1)} %copy-done.6, f32[1024]{0:T(1024)S(1)} %add_rsqrt_fusion), kind=kOutput, calls=%fused_computation.36 | convolution fusion | flops 4304404480 | bytes 10498048 | tf_op jit(solution)/shard_map/dot_general | solution.py:352
  207.0 1.0 fusion.27
  208.0 1.2 subtract_convert_fusion
  209.3 0.4 copy.30
  209.7 0.9 copy.43
  210.6 1.4 copy.31
  212.0 1.3 copy.39
  213.2 1.6 copy.34
  214.9 0.3 fusion.22
  215.3 0.7 copy-done.2
  216.1 0.6 fusion.23
  216.6 7.1 %while.13 = (s32[]{:T(128)}, f32[2,128,256]{2,1,0:T(8,128)S(1)}, f32[8,2,128,256]{3,2,1,0:T(8,128)}, f32[8,2,128,256]{3,2,1,0:T(8,128)S(1)}, s32[]{:T(128)}, /*index=5*/s32[]{:T(128)}, s32[]{:T(128)}) while((s32[]{:T(128)}, f32[2,128,256]{2,1,0:T(8,128)S(1)}, f32[8,2,128,256]{3,2,1,0:T(8,128)}, f32[8,2,128,256]{3,2,1,0:T(8,128)S(1)}, ...), condition=%wide.region_2.3_spmd.clone, body=%wide.region_1.2_spmd.clone.sunk | while | flops 262155 | bytes 1311344 | solution.py:287
  216.6 0.7 bitcast_dynamic-update-slice_fusion.2
  217.5 0.7 bitcast_dynamic-update-slice_fusion.2
  218.4 0.7 bitcast_dynamic-update-slice_fusion.2
  219.2 0.7 bitcast_dynamic-update-slice_fusion.2
  220.1 0.7 bitcast_dynamic-update-slice_fusion.2
  221.0 0.7 bitcast_dynamic-update-slice_fusion.2
  221.8 0.7 bitcast_dynamic-update-slice_fusion.2
  222.7 0.7 bitcast_dynamic-update-slice_fusion.2
  223.7 1.0 copy.40
  224.7 0.3 copy.28
  225.1 1.2 copy.41
  226.2 0.3 copy.29
  226.7 5.2 %fusion.28 = f32[8,2,256,128]{3,2,1,0:T(8,128)} fusion(f32[8,2,128,256]{3,2,1,0:T(8,128)} %get-tuple-element.40, bf16[8,128,2,64]{3,1,2,0:T(8,128)(2,1)S(1)} %copy.29, bf16[8,128,2,64]{3,1,2,0:T(8,128)(2,1)S(1)} %copy.28), kind=kOutput, calls=%fused_computation.56 | convolution fusion | flops 806354944 | bytes 4718592 | tf_op jit(solution)/shard_map/cihd,chde->cihe/dot_general | solution.py:290
  231.8 3.0 fusion.39
  234.9 2.5 copy.36
  237.4 0.2 multiply_reduce_fusion
  237.7 2.1 fusion.16
  239.8 5.9 %convolution_convert_fusion.3 = bf16[1024,2048]{1,0:T(8,128)(2,1)} fusion(bf16[1024,512]{0,1:T(8,128)(2,1)S(1)} %fusion.16, bf16[512,2048]{1,0:T(8,128)(2,1)} %get-tuple-element.41), kind=kOutput, calls=%fused_computation.27 | convolution fusion | flops 2149580800 | bytes 7340032 | tf_op jit(solution)/shard_map/dot_general | solution.py:364
  245.7 1.7 constant_dynamic-slice_fusion.1
  247.6 4.3 %collective-permute-done = bf16[512,2048]{1,0:T(8,128)(2,1)} collective-permute-done((bf16[512,2048]{1,0:T(8,128)(2,1)S(1)}, bf16[512,2048]{1,0:T(8,128)(2,1)}, u32[]{:S(2)}, u32[]{:S(2)}) %collective-permute-start) | collective-permute-done | bytes 2097184 | tf_op jit(solution)/shard_map/ppermute | solution.py:317
  251.8 4.1 %fusion.5 = (f32[512]{0:T(512)S(1)}, bf16[512,2048]{1,0:T(8,128)(2,1)S(1)}) fusion(bf16[512,2048]{1,0:T(8,128)(2,1)} %collective-permute-done, bf16[1024,2048]{1,0:T(8,128)(2,1)} %convolution_convert_fusion.3, s32[]{:T(128)S(6)} %select_n.33, bf16[512,2048]{1,0:T(8,128)(2,1)} %refs_0_.1), kind=kLoop, calls=%fused_computation.13 | loop fusion | flops 9436672 | bytes 8390660 | tf_op jit(solution)/shard_map/reduce_sum | solution.py:244
  256.0 1.9 fusion.7
  258.0 1.0 dynamic-slice_reduce_fusion.2
  259.0 3.4 %collective-permute-done.1 = bf16[512,2048]{1,0:T(8,128)(2,1)} collective-permute-done((bf16[512,2048]{1,0:T(8,128)(2,1)}, bf16[512,2048]{1,0:T(8,128)(2,1)}, u32[]{:S(2)}, u32[]{:S(2)}) %collective-permute-start.1) | collective-permute-done | bytes 2097184 | tf_op jit(solution)/shard_map/ppermute | solution.py:322
  262.3 3.2 broadcast_select_fusion.1
  265.5 10.7 %fusion.14 = f32[1024,1408]{1,0:T(8,128)} fusion(bf16[2048,1408]{1,0:T(8,128)(2,1)} %get-tuple-element.42, bf16[512,2048]{1,0:T(8,128)(2,1)S(1)} %get-tuple-element.85, bf16[512,2048]{1,0:T(8,128)(2,1)S(1)} %get-tuple-element.84), kind=kOutput, calls=%fused_computation.25 | convolution fusion | flops 5916852224 | bytes 15728640 | tf_op jit(solution)/shard_map/dot_general | solution.py:370
  276.2 9.6 %fusion.13 = f32[1024,1408]{1,0:T(8,128)} fusion(bf16[2048,1408]{1,0:T(8,128)(2,1)S(1)} %bitcast.93, bf16[512,2048]{1,0:T(8,128)(2,1)S(1)} %get-tuple-element.85, bf16[512,2048]{1,0:T(8,128)(2,1)S(1)} %get-tuple-element.84), kind=kOutput, calls=%fused_computation.23 | convolution fusion | flops 5916852224 | bytes 15728640 | tf_op jit(solution)/shard_map/dot_general | solution.py:371
  285.8 22.7 %convolution_convert_fusion.2 = bf16[1024,2048]{1,0:T(8,128)(2,1)} fusion(bf16[1408,2048]{1,0:T(8,128)(2,1)} %get-tuple-element.44, f32[1024,1408]{1,0:T(8,128)} %fusion.13, f32[1024,1408]{1,0:T(8,128)} %fusion.14, f32[1408]{0:T(1024)S(1)} %get-tuple-element.71, f32[1408]{0:T(1024)S(1)} %get-tuple-element.70, f32[1408]{0:T(1024)S(1)} %get-tuple-element.69, ...), kind=kOutput, calls=%fused_computation.26 | convolution fusion | flops 5930745856 | bytes 21529600 | tf_op jit(solution)/shard_map/dot_general | solution.py:378
  308.5 1.9 constant_dynamic-slice_fusion
  310.4 0.2 collective-permute-start.2
  310.6 4.0 %collective-permute-done.2 = bf16[512,2048]{1,0:T(8,128)(2,1)S(1)} collective-permute-done((bf16[512,2048]{1,0:T(8,128)(2,1)S(1)}, bf16[512,2048]{1,0:T(8,128)(2,1)S(1)}, u32[]{:S(2)}, u32[]{:S(2)}) %collective-permute-start.2) | collective-permute-done | bytes 2097184 | tf_op jit(solution)/shard_map/ppermute | solution.py:317
  314.6 2.6 fusion.8
  (53 shorter events, 1.9 us)
Async XLA Ops:
  1.9 197.0 %copy-start.6 = (f32[2048]{0:T(1024)S(1)}, f32[2048]{0:T(1024)}, u32[]{:S(2)}) copy-start(f32[2048]{0:T(1024)} %param.15) | copy-start | bytes 24580
  195.6 3.5 %copy-start.3 = (bf16[1024,2048]{1,0:T(8,128)(2,1)S(1)}, bf16[1024,2048]{1,0:T(8,128)(2,1)}, u32[]{:S(2)}) copy-start(bf16[1024,2048]{1,0:T(8,128)(2,1)} %get-tuple-element.38) | copy-start | bytes 12582916
  215.2 0.8 copy-start.2
  225.1 6.8 %copy-start = (bf16[8,128,2,64]{3,1,2,0:T(8,128)(2,1)}, bf16[8,128,2,64]{3,1,2,0:T(8,128)(2,1)S(1)}, u32[]{:S(2)}) copy-start(bf16[8,128,2,64]{3,1,2,0:T(8,128)(2,1)S(1)} %copy.28) | copy-start | bytes 786436
  226.6 5.3 %copy-start.1 = (bf16[8,128,2,64]{3,1,2,0:T(8,128)(2,1)}, bf16[8,128,2,64]{3,1,2,0:T(8,128)(2,1)S(1)}, u32[]{:S(2)}) copy-start(bf16[8,128,2,64]{3,1,2,0:T(8,128)(2,1)S(1)} %copy.29) | copy-start | bytes 786436
  247.5 4.4 %collective-permute-start = (bf16[512,2048]{1,0:T(8,128)(2,1)S(1)}, bf16[512,2048]{1,0:T(8,128)(2,1)}, u32[]{:S(2)}, u32[]{:S(2)}) collective-permute-start(bf16[512,2048]{1,0:T(8,128)(2,1)S(1)} %constant_dynamic-slice_fusion.1), channel_id=1, source_target_pairs={{0,1},{1,0},{2,3},{3,2},{4,5},{5,4},{6,7},{7,6},{8,9},{9,8},{10,11... | collective-permute-start | bytes 6291464 | tf_op jit(solution)/shard_map/ppermute | solution.py:317
  247.5 8.4 %copy-start.5 = (f32[2048]{0:T(1024)S(1)}, f32[2048]{0:T(1024)}, u32[]{:S(2)}) copy-start(f32[2048]{0:T(1024)} %param.20) | copy-start | bytes 24580
  257.8 4.5 %collective-permute-start.1 = (bf16[512,2048]{1,0:T(8,128)(2,1)}, bf16[512,2048]{1,0:T(8,128)(2,1)}, u32[]{:S(2)}, u32[]{:S(2)}) collective-permute-start(bf16[512,2048]{1,0:T(8,128)(2,1)} %fusion.7), channel_id=1, source_target_pairs={{0,1},{1,0},{2,3},{3,2},{4,5},{5,4},{6,7},{7,6},{8,9},{9,8},{10,11... | collective-permute-start | bytes 6291464 | tf_op jit(solution)/shard_map/ppermute | solution.py:322
  262.3 13.9 %slice-start = ((s8[5767168]{0:T(1024)(128)(4,1)}), s8[4194304]{0:T(1024)(128)(4,1)S(1)}, s32[]{:S(2)}) async-start(s8[5767168]{0:T(1024)(128)(4,1)} %bitcast.92), calls=%async_computation | async-start | bytes 8388608
  265.5 10.7 %slice-start.1 = ((s8[5767168]{0:T(1024)(128)(4,1)}), s8[1572864]{0:T(1024)(128)(4,1)S(1)}, s32[]{:S(2)}) async-start(s8[5767168]{0:T(1024)(128)(4,1)} %bitcast.92), calls=%async_computation.1 | async-start | bytes 3145728
  308.5 6.1 %copy-start.4 = (bf16[1024,2048]{1,0:T(8,128)(2,1)S(1)}, bf16[1024,2048]{1,0:T(8,128)(2,1)}, u32[]{:S(2)}) copy-start(bf16[1024,2048]{1,0:T(8,128)(2,1)} %convolution_convert_fusion.2) | copy-start | bytes 12582916
  310.4 4.2 %collective-permute-start.2 = (bf16[512,2048]{1,0:T(8,128)(2,1)S(1)}, bf16[512,2048]{1,0:T(8,128)(2,1)S(1)}, u32[]{:S(2)}, u32[]{:S(2)}) collective-permute-start(bf16[512,2048]{1,0:T(8,128)(2,1)S(1)} %constant_dynamic-slice_fusion), channel_id=1, source_target_pairs={{0,1},{1,0},{2,3},{3,2},{4,5},{5,4},{6,7},{7,6},{8,9},{9,8},{10,11... | collective-permute-start | bytes 6291464 | tf_op jit(solution)/shard_map/ppermute | solution.py:317

commit v2 on v1

--- a/solution.py
+++ b/solution.py
@@ -25,10 +25,11 @@
     count = len(kinds)
     tokens = refs[0]
     shards = refs[1 : 1 + count]
-    both = refs[1 + count]
-    fulls = refs[2 + count : 2 + 2 * count]
-    (tok_sems, own_sems, up_send, up_recv, down_send, down_recv, y_send, y_recv, x_send, x_recv) = refs[
-        2 + 2 * count :
+    gain, cosine, sine, inside, tail, onset, passing = refs[1 + count : 8 + count]
+    hidden = refs[8 + count]
+    fulls = (refs[8 + 2 * count],) + tuple(refs[9 + count : 8 + 2 * count])
+    (both, state, tok_sems, own_sems, up_send, up_recv, down_send, down_recv, y_send, y_recv, x_send, x_recv) = refs[
+        9 + 2 * count :
     ]
     depth = fs // 2
     rep = lax.axis_index("rep")
@@ -173,43 +174,103 @@
         take_y(p, s + 1)
         take_y(p, depth + s)
 
-    lag = 2
-    total = len(events)
-    start_z(*events[0])
-    for e in range(total + lag):
-        if e < total:
-            take_z(*events[e])
-            if e + 1 < total:
-                start_z(*events[e + 1])
-            spread(*events[e])
-        if e >= lag:
-            finish_y(*events[e - lag])
-
-    for p in range(count):
+    heads = state.shape[0]
+
+    def ready():
         for k in range(kmax):
 
             @pl.when(valid(k))
             def _():
                 if k > 0:
-                    x_copy(p, k, 0, False).wait_recv()
+                    x_copy(0, k, 0, False).wait_recv()
+                x_copy(0, k, 1, False).wait_recv()
+
+        owns[0].wait()
+        tok_own.wait()
+        tok_out.wait()
+        state[...] = jnp.zeros_like(state)
+
+    def attend(c):
+        span = pl.ds(c * BLOCK, BLOCK)
+        values = both[span, :].astype(jnp.float32)
+        factor = lax.rsqrt(jnp.mean(values * values, axis=-1, keepdims=True) + epsilon)
+        normed = (values * factor * gain[...]).astype(jnp.bfloat16)
+        joined = jnp.dot(normed, fulls[0][...], preferred_element_type=jnp.float32).astype(jnp.bfloat16)
+        cos, sin = cosine[span, :], sine[span, :]
+
+        def rotate(matrix):
+            wide = matrix.astype(jnp.float32)
+            return wide * cos + pltpu.roll(wide, DK // 2, 1) * sin
+
+        for h in range(heads):
+            query = rotate(joined[:, h * DK : (h + 1) * DK]).astype(jnp.bfloat16)
+            key = joined[:, (heads + h) * DK : (heads + h + 1) * DK]
+            key = (rotate(key) * DK ** (-0.5)).astype(jnp.bfloat16)
+            first = 2 * heads * DK + h * DV
+            value = joined[:, first : first + DV]
+            scores = lax.dot_general(query, key, (((1,), (1,)), ((), ())), preferred_element_type=jnp.float32)
+            weights = (scores * inside[h]).astype(jnp.bfloat16)
+            inner = jnp.dot(weights, value, preferred_element_type=jnp.float32)
+            cross = jnp.dot(
+                query.astype(jnp.float32),
+                state[h],
+                precision=lax.Precision.HIGHEST,
+                preferred_element_type=jnp.float32,
+            )
+            retained = inner + cross * onset[h]
+            decayed = (key.astype(jnp.float32) * tail[h]).astype(jnp.bfloat16)
+            fresh = lax.dot_general(decayed, value, (((0,), (0,)), ((), ())), preferred_element_type=jnp.float32)
+            state[h] = state[h] * passing[h] + fresh
+            hidden[span, h * DV : (h + 1) * DV] = head_norm(retained).astype(jnp.bfloat16)
+
+    lag = 2
+    first_block = steps + lag + 1
+    blocks = both.shape[0] // BLOCK
+    total = len(events)
+    start_z(*events[0])
+    for e in range(max(total + lag, first_block + blocks)):
+        if e < total:
+            p, s = events[e]
+            if s == steps - 2 and p + 1 < count:
+                start_z(p + 1, 0)
+            take_z(p, s)
+            if s + 1 < steps:
+                start_z(p, s + 1)
+            spread(p, s)
+        if lag <= e < total + lag:
+            finish_y(*events[e - lag])
+        if e == first_block:
+            ready()
+        if first_block <= e < first_block + blocks:
+            attend(e - first_block)
+
+    for p in range(count):
+        for k in range(kmax):
+
+            @pl.when(valid(k))
+            def _():
+                if k > 0:
+                    if p > 0:
+                        x_copy(p, k, 0, False).wait_recv()
                     x_copy(p, k, 0, True).wait_send()
-                x_copy(p, k, 1, False).wait_recv()
+                if p > 0:
+                    x_copy(p, k, 1, False).wait_recv()
                 x_copy(p, k, 1, True).wait_send()
                 y_copy(p, k).wait_send()
 
         for s in range(steps):
             pl.when((z - s >= 0) & (z < depth - 1))(lambda: up(p, s).wait_send())
             pl.when((z + s <= depth - 1) & (z > 0))(lambda: down(p, s).wait_send())
-    for own in owns:
+    for own in owns[1:]:
         own.wait()
-    tok_own.wait()
-    tok_out.wait()
-
-
-def gather_all(sizes, tokens, shards):
+
+
+def gather_all(sizes, tokens, shards, tables):
     fs = sizes[1]
     kinds = []
-    outs = [jax.ShapeDtypeStruct((tokens.shape[0] * 2, tokens.shape[1]), tokens.dtype)]
+    length = tokens.shape[0] * 2
+    heads = tables[3].shape[0]
+    outs = [jax.ShapeDtypeStruct((length, heads * DV), jnp.bfloat16)]
     for shard, by_cols in shards:
         rows, cols = shard.shape
         side = by_cols and cols % 128 == 0
@@ -221,17 +282,23 @@
     anywhere = pl.BlockSpec(memory_space=pl.ANY)
     got = pl.pallas_call(
         functools.partial(gather_kernel, sizes, tuple(kinds)),
-        out_shape=outs,
-        in_specs=[vmem] * (count + 1),
-        out_specs=[anywhere] * (count + 1),
-        scratch_shapes=[dma((3,)), dma((count,))]
+        out_shape=outs[:1] + outs[2:],
+        in_specs=[vmem] * (count + 1 + len(tables)),
+        out_specs=[vmem] + [anywhere] * (count - 1),
+        scratch_shapes=[
+            pltpu.VMEM(outs[1].shape, outs[1].dtype),
+            pltpu.VMEM((length, tokens.shape[1]), tokens.dtype),
+            pltpu.VMEM((heads, DK, DV), jnp.float32),
+            dma((3,)),
+            dma((count,)),
+        ]
         + [dma((count, depth - 1))] * 4
         + [dma((count, 2 * depth - 1))] * 2
         + [dma((count, 4 * depth - 2))] * 2,
         compiler_params=pltpu.CompilerParams(collective_id=0, has_side_effects=True),
-    )(tokens, *[shard for shard, _ in shards])
+    )(tokens, *[shard for shard, _ in shards], *tables)
     fulls = []
-    for full, (shard, by_cols), kind in zip(got[1:], shards, kinds):
+    for full, (shard, by_cols), kind in zip(got[1:], shards[1:], kinds[1:]):
         if by_cols and kind == ROWS:
             rows, cols = shard.shape
             full = full.reshape(fs, rows, cols).transpose(1, 0, 2).reshape(rows, fs * cols)
@@ -245,54 +312,30 @@
     return (values * factor * scale_vec).astype(jnp.bfloat16)
 
 
-def rotate_heads(matrix):
-    length = matrix.shape[0]
-    half_width = matrix.shape[-1] // 2
+def rotation(length):
+    half_width = DK // 2
     inverse = 10000.0 ** (-jnp.arange(half_width, dtype=jnp.float32) * 2.0 / (2 * half_width))
     angles = jnp.arange(length, dtype=jnp.float32)[:, None] * inverse[None, :]
-    cosine = jnp.cos(angles)[:, None, :]
-    sine = jnp.sin(angles)[:, None, :]
-    values = matrix.astype(jnp.float32)
-    first_half = values[..., :half_width]
-    second_half = values[..., half_width:]
-    return jnp.concatenate(
-        [first_half * cosine - second_half * sine, first_half * sine + second_half * cosine],
-        axis=-1,
-    )
-
-
-def retain_blocks(rot_query, rot_key, value, rates, block_len):
-    length, head_count, width_k = rot_query.shape
-    width_v = value.shape[-1]
-    blocks = length // block_len
-    query4 = rot_query.reshape(blocks, block_len, head_count, width_k)
-    key4 = rot_key.reshape(blocks, block_len, head_count, width_k)
-    value4 = value.reshape(blocks, block_len, head_count, width_v)
+    cosine, sine = jnp.cos(angles), jnp.sin(angles)
+    return jnp.concatenate([cosine, cosine], axis=1), jnp.concatenate([-sine, sine], axis=1)
+
+
+def decays(rates, block_len):
+    heads = rates.shape[0]
     places = jnp.arange(block_len, dtype=jnp.float32)
     spacing = places[:, None] - places[None, :]
     inside = jnp.where(
         spacing[None] >= 0, jnp.exp(-jnp.maximum(spacing, 0.0)[None] * rates[:, None, None]), 0.0
     )
-    scores = jnp.einsum("cihd,cjhd->chij", query4, key4, preferred_element_type=jnp.float32)
-    weights = (scores * inside[None]).astype(jnp.bfloat16)
-    inner_part = jnp.einsum("chij,cjhe->cihe", weights, value4, preferred_element_type=jnp.float32)
-    tail_decay = jnp.exp(-(block_len - 1.0 - places)[:, None] * rates[None, :])
-    decayed = (key4.astype(jnp.float32) * tail_decay[None, :, :, None]).astype(jnp.bfloat16)
-    states = jnp.einsum("cjhd,cjhe->chde", decayed, value4, preferred_element_type=jnp.float32)
+    tail = jnp.exp(-(block_len - 1.0 - places)[None, :, None] * rates[:, None, None])
+    onset = jnp.exp(-(places + 1.0)[None, :, None] * rates[:, None, None])
     passing = jnp.exp(-block_len * rates)[:, None, None]
-
-    def advance(carried, fresh):
-        return (carried * passing + fresh, carried)
-
-    _, before = lax.scan(advance, jnp.zeros((head_count, width_k, width_v), jnp.float32), states)
-    onset_decay = jnp.exp(-(places + 1.0)[:, None] * rates[None, :])
-    cross_part = (
-        jnp.einsum(
-            "cihd,chde->cihe", query4.astype(jnp.float32), before, precision=lax.Precision.HIGHEST
-        )
-        * onset_decay[None, :, :, None]
-    )
-    return (inner_part + cross_part).reshape(length, head_count, width_v)
+    return (
+        inside,
+        jnp.broadcast_to(tail, (heads, block_len, DK)),
+        jnp.broadcast_to(onset, (heads, block_len, DV)),
+        jnp.broadcast_to(passing, (heads, 1, DV)),
+    )
 
 
 def head_norm(retained):
@@ -343,23 +386,15 @@
     heads_here = w_query.shape[1] // DK
     qk_cols = w_query.shape[1]
     qkv_shard = jnp.concatenate([w_query, w_key, w_value], axis=1)
-    both, (qkv_w, out_full, gate_w, up_w, down_full) = gather_all(
+    length = tokens.shape[0] * 2
+    head_ids = (tp_rank * heads_here + jnp.arange(heads_here, dtype=jnp.int32)).astype(jnp.float32)
+    rates = 1.0 / 16.0 * (32.0 / LENGTH) ** (head_ids / (HEADS - 1))
+    hidden, (out_full, gate_w, up_w, down_full) = gather_all(
         sizes,
         tokens,
         ((qkv_shard, False), (w_out, True), (w_ffgate, False), (w_ffup, False), (w_down, True)),
-    )
-    pieces = rms_rows(both, mix_gain)
-    joined = jnp.dot(pieces, qkv_w, preferred_element_type=jnp.float32).astype(jnp.bfloat16)
-    length = joined.shape[0]
-    query = joined[:, :qk_cols].reshape(length, heads_here, DK)
-    key = joined[:, qk_cols : 2 * qk_cols].reshape(length, heads_here, DK)
-    value = joined[:, 2 * qk_cols :].reshape(length, heads_here, DV)
-    rot_query = rotate_heads(query).astype(jnp.bfloat16)
-    rot_key = (rotate_heads(key) * DK ** (-0.5)).astype(jnp.bfloat16)
-    head_ids = (tp_rank * heads_here + jnp.arange(heads_here, dtype=jnp.int32)).astype(jnp.float32)
-    rates = 1.0 / 16.0 * (32.0 / LENGTH) ** (head_ids / (HEADS - 1))
-    retained = retain_blocks(rot_query, rot_key, value, rates, BLOCK)
-    hidden = head_norm(retained).reshape(length, heads_here * DV).astype(jnp.bfloat16)
+        (mix_gain[None, :],) + rotation(length) + decays(rates, BLOCK),
+    )
     mix_sum = sum_over_tp(
         jnp.dot(hidden, out_full, preferred_element_type=jnp.float32).astype(jnp.bfloat16), tp_rank
     )

time: 318 us -> 279 us (0.88)
  matrix products: 65.1 us -> 48.8 us
  other arithmetic: 28.9 us -> 16.8 us
  local copies, waits for them, and re-layouts: 16.7 us -> 6.84 us
    dot_general x4 -> x0, matrix products: 16.2 us -> none  [the longest x1 7.45 us: body(): jnp.dot(pieces, qkv_w, preferred_element_type=jnp.float32)]
    dynamic_update_slice x8 -> x0, other arithmetic: 5.81 us -> none  [retain_blocks(): lax.scan(advance, jnp.zeros((head_count, width_k, width_v), jnp.float32),...]
    unnamed x24 -> x14, local copies, waits for them, and re-layouts: 5.44 us -> 0.03 us
    reduce_sum x2 -> x1, other arithmetic: 7.34 us -> 4.12 us  [rms_rows(): jnp.mean(values * values, axis=-1, keepdims=True) + epsilon]
where the time goes in v2:
time: 279 us
  Pallas kernels  194 us (70%)
  matrix products  48.8 us (17%)
  other arithmetic  16.8 us (6%)
  waiting for transfers between devices  11.7 us (4%)
  local copies, waits for them, and re-layouts  6.84 us (2%)
    pallas_call x1, Pallas kernels, gather_all(): pl.pallas_call(functools.partial(gather_kernel, sizes, tuple(kinds)), out...  194 us
    dot_general x1, matrix products, body(): jnp.dot(activ, down_full, preferred_element_type=jnp.float32)  22.6 us
    dot_general x1, matrix products, body(): jnp.dot(pieces, gate_w, preferred_element_type=jnp.float32)  10.4 us
    dot_general x1, matrix products, body(): jnp.dot(pieces, up_w, preferred_element_type=jnp.float32)  9.64 us
    ppermute x2, waiting for transfers between devices, sum_over_tp(): got = lax.ppermute(theirs, 'tp', [(0, 1), (1, 0)])  8.28 us
    dot_general x1, matrix products, body(): jnp.dot(hidden, out_full, preferred_element_type=jnp.float32)  6.22 us
  transfers between devices with their start and end apart: 3, of which 3 were waited for; matrix products, arithmetic and copies ran while one was open for 0% of the time, Pallas kernels for 0%

profile of v2, /device:TPU:0, one launch (start us, length us, event | category | flops | bytes accessed | tf_op | source)
XLA Modules:
  0.0 278.7 jit_solution(6762253424684183525)
XLA Ops:
  0.0 0.0 copy-start.3
  0.0 0.0 copy-start.2
  0.0 0.0 copy-start.1
  0.1 2.0 fusion.8
  2.1 0.1 multiply_exponential_fusion
  2.2 0.8 exponential_select_fusion.refs_9_
  2.9 1.3 pad_maximum_fusion.4
  4.2 0.0 copy-done.3
  4.2 0.0 copy-done.2
  4.2 0.0 copy-done.1
  4.3 0.9 pad_maximum_fusion.3.refs_1_
  5.1 0.8 broadcast_in_dim.24.refs_11_
  5.9 0.7 broadcast_in_dim.23.refs_10_
  6.7 0.7 broadcast_in_dim.25.refs_12_
  7.3 194.1 %shard_map.118 = (bf16[1024,512]{1,0:T(8,128)(2,1)}, bf16[512,2048]{1,0:T(8,128)(2,1)}, bf16[2048,1408]{1,0:T(8,128)(2,1)}, bf16[2048,1408]{1,0:T(8,128)(2,1)}, bf16[1408,2048]{1,0:T(8,128)(2,1)}) custom-call(bf16[512,2048]{1,0:T(8,128)(2,1)} %refs_0_.1, bf16[256,1024]{1,0:T(8,128)(2,1)} %pad_maximum_fusion.3.refs_1_, bf16[512,256]{1,0:T(8,128)(2,1)} %refs_2_.1, ...), custom_call_target="tpu_custom_call" | custom-call | tf_op jit(solution)/shard_map/pallas_call | solution.py:283
  201.4 6.2 %convolution_convert_fusion.3 = bf16[1024,2048]{1,0:T(8,128)(2,1)} fusion(bf16[1024,512]{1,0:T(8,128)(2,1)} %get-tuple-element.10, bf16[512,2048]{1,0:T(8,128)(2,1)} %get-tuple-element.11), kind=kOutput, calls=%fused_computation.15 | convolution fusion | flops 2149580800 | bytes 7340032 | tf_op jit(solution)/shard_map/dot_general | solution.py:399
  207.7 1.7 constant_dynamic-slice_fusion.1
  209.4 0.1 collective-permute-start
  209.5 0.0 copy-start.4
  209.5 4.3 %collective-permute-done = bf16[512,2048]{1,0:T(8,128)(2,1)} collective-permute-done((bf16[512,2048]{1,0:T(8,128)(2,1)S(1)}, bf16[512,2048]{1,0:T(8,128)(2,1)}, u32[]{:S(2)}, u32[]{:S(2)}) %collective-permute-start) | collective-permute-done | bytes 2097184 | tf_op jit(solution)/shard_map/ppermute | solution.py:360
  213.7 4.1 %fusion = (f32[512]{0:T(512)S(1)}, bf16[512,2048]{1,0:T(8,128)(2,1)S(1)}) fusion(bf16[512,2048]{1,0:T(8,128)(2,1)} %collective-permute-done, bf16[1024,2048]{1,0:T(8,128)(2,1)} %convolution_convert_fusion.3, s32[]{:T(128)S(6)} %select_n.29, bf16[512,2048]{1,0:T(8,128)(2,1)} %refs_0_.1), kind=kLoop, calls=%fused_computation.4 | loop fusion | flops 9436672 | bytes 8390660 | tf_op jit(solution)/shard_map/reduce_sum | solution.py:311
  217.9 0.0 copy-done.4
  217.9 1.9 fusion.2
  219.7 0.1 collective-permute-start.1
  219.9 1.0 dynamic-slice_reduce_fusion.2
  220.9 3.4 %collective-permute-done.1 = bf16[512,2048]{1,0:T(8,128)(2,1)} collective-permute-done((bf16[512,2048]{1,0:T(8,128)(2,1)}, bf16[512,2048]{1,0:T(8,128)(2,1)}, u32[]{:S(2)}, u32[]{:S(2)}) %collective-permute-start.1) | collective-permute-done | bytes 2097184 | tf_op jit(solution)/shard_map/ppermute | solution.py:365
  224.2 0.0 slice-start
  224.2 3.2 %broadcast_select_fusion.1 = (bf16[512,2048]{1,0:T(8,128)(2,1)S(1)}, bf16[512,2048]{1,0:T(8,128)(2,1)S(1)}) fusion(bf16[512,2048]{1,0:T(8,128)(2,1)} %collective-permute-done.1, pred[]{:T(512)S(6)} %eq.3, f32[2048]{0:T(1024)S(1)} %copy-done.4, f32[512]{0:T(512)S(1)} %add_rsqrt_fusion, bf16[512,2048]{1,0:T(8,128)(2,1)S(1)} %get-tuple-element.22), kind=kLoop, calls=%fused_computation.17 | loop fusion | flops 6291456 | bytes 8398849 | tf_op jit(solution)/shard_map/jit(_where)/select_n | solution.py:367
  227.4 0.0 slice-start.1
  227.4 10.4 %fusion.5 = f32[1024,1408]{1,0:T(8,128)} fusion(bf16[2048,1408]{1,0:T(8,128)(2,1)} %get-tuple-element.12, bf16[512,2048]{1,0:T(8,128)(2,1)S(1)} %get-tuple-element.24, bf16[512,2048]{1,0:T(8,128)(2,1)S(1)} %get-tuple-element.23), kind=kOutput, calls=%fused_computation.13 | convolution fusion | flops 5916852224 | bytes 15728640 | tf_op jit(solution)/shard_map/dot_general | solution.py:405
  237.8 0.0 slice-done
  237.8 0.0 slice-done.1
  237.8 9.6 %fusion.4 = f32[1024,1408]{1,0:T(8,128)} fusion(bf16[2048,1408]{1,0:T(8,128)(2,1)S(1)} %bitcast.8, bf16[512,2048]{1,0:T(8,128)(2,1)S(1)} %get-tuple-element.24, bf16[512,2048]{1,0:T(8,128)(2,1)S(1)} %get-tuple-element.23), kind=kOutput, calls=%fused_computation.11 | convolution fusion | flops 5916852224 | bytes 15728640 | tf_op jit(solution)/shard_map/dot_general | solution.py:406
  247.5 22.6 %convolution_convert_fusion.2 = bf16[1024,2048]{1,0:T(8,128)(2,1)} fusion(bf16[1408,2048]{1,0:T(8,128)(2,1)} %get-tuple-element.14, f32[1024,1408]{1,0:T(8,128)} %fusion.4, f32[1024,1408]{1,0:T(8,128)} %fusion.5, f32[1408]{0:T(1024)S(1)} %get-tuple-element.20, f32[1408]{0:T(1024)S(1)} %get-tuple-element.19, f32[1408]{0:T(1024)S(1)} %get-tuple-element.18, ...), kind=kOutput, calls=%fused_computation.14 | convolution fusion | flops 5930745856 | bytes 21529600 | tf_op jit(solution)/shard_map/dot_general | solution.py:413
  270.0 0.0 copy-start
  270.0 1.9 constant_dynamic-slice_fusion
  271.9 0.2 collective-permute-start.2
  272.1 4.0 %collective-permute-done.2 = bf16[512,2048]{1,0:T(8,128)(2,1)S(1)} collective-permute-done((bf16[512,2048]{1,0:T(8,128)(2,1)S(1)}, bf16[512,2048]{1,0:T(8,128)(2,1)S(1)}, u32[]{:S(2)}, u32[]{:S(2)}) %collective-permute-start.2) | collective-permute-done | bytes 2097184 | tf_op jit(solution)/shard_map/ppermute | solution.py:360
  276.1 0.0 copy-done
  276.1 2.6 fusion.3
  (7 shorter events, 0.1 us)
Async XLA Ops:
  0.0 4.2 %copy-start.3 = (bf16[256,256]{1,0:T(8,128)(2,1)S(1)}, bf16[256,256]{1,0:T(8,128)(2,1)}, u32[]{:S(2)}) copy-start(bf16[256,256]{1,0:T(8,128)(2,1)} %param.14) | copy-start | bytes 393220
  0.0 4.2 %copy-start.2 = (bf16[256,256]{1,0:T(8,128)(2,1)S(1)}, bf16[256,256]{1,0:T(8,128)(2,1)}, u32[]{:S(2)}) copy-start(bf16[256,256]{1,0:T(8,128)(2,1)} %param.15) | copy-start | bytes 393220
  0.0 4.2 %copy-start.1 = (bf16[256,512]{1,0:T(8,128)(2,1)S(1)}, bf16[256,512]{1,0:T(8,128)(2,1)}, u32[]{:S(2)}) copy-start(bf16[256,512]{1,0:T(8,128)(2,1)} %param.16) | copy-start | bytes 786436
  209.4 4.4 %collective-permute-start = (bf16[512,2048]{1,0:T(8,128)(2,1)S(1)}, bf16[512,2048]{1,0:T(8,128)(2,1)}, u32[]{:S(2)}, u32[]{:S(2)}) collective-permute-start(bf16[512,2048]{1,0:T(8,128)(2,1)S(1)} %constant_dynamic-slice_fusion.1), channel_id=1, source_target_pairs={{0,1},{1,0},{2,3},{3,2},{4,5},{5,4},{6,7},{7,6},{8,9},{9,8},{10,11... | collective-permute-start | bytes 6291464 | tf_op jit(solution)/shard_map/ppermute | solution.py:360
  209.5 8.4 %copy-start.4 = (f32[2048]{0:T(1024)S(1)}, f32[2048]{0:T(1024)}, u32[]{:S(2)}) copy-start(f32[2048]{0:T(1024)} %param.18) | copy-start | bytes 24580
  219.7 4.5 %collective-permute-start.1 = (bf16[512,2048]{1,0:T(8,128)(2,1)}, bf16[512,2048]{1,0:T(8,128)(2,1)}, u32[]{:S(2)}, u32[]{:S(2)}) collective-permute-start(bf16[512,2048]{1,0:T(8,128)(2,1)} %fusion.2), channel_id=1, source_target_pairs={{0,1},{1,0},{2,3},{3,2},{4,5},{5,4},{6,7},{7,6},{8,9},{9,8},{10,11... | collective-permute-start | bytes 6291464 | tf_op jit(solution)/shard_map/ppermute | solution.py:365
  224.2 13.6 %slice-start = ((s8[5767168]{0:T(1024)(128)(4,1)}), s8[4194304]{0:T(1024)(128)(4,1)S(1)}, s32[]{:S(2)}) async-start(s8[5767168]{0:T(1024)(128)(4,1)} %bitcast.7), calls=%async_computation | async-start | bytes 8388608
  227.4 10.4 %slice-start.1 = ((s8[5767168]{0:T(1024)(128)(4,1)}), s8[1572864]{0:T(1024)(128)(4,1)S(1)}, s32[]{:S(2)}) async-start(s8[5767168]{0:T(1024)(128)(4,1)} %bitcast.7), calls=%async_computation.1 | async-start | bytes 3145728
  270.0 6.1 %copy-start = (bf16[1024,2048]{1,0:T(8,128)(2,1)S(1)}, bf16[1024,2048]{1,0:T(8,128)(2,1)}, u32[]{:S(2)}) copy-start(bf16[1024,2048]{1,0:T(8,128)(2,1)} %convolution_convert_fusion.2) | copy-start | bytes 12582916
  271.9 4.2 %collective-permute-start.2 = (bf16[512,2048]{1,0:T(8,128)(2,1)S(1)}, bf16[512,2048]{1,0:T(8,128)(2,1)S(1)}, u32[]{:S(2)}, u32[]{:S(2)}) collective-permute-start(bf16[512,2048]{1,0:T(8,128)(2,1)S(1)} %constant_dynamic-slice_fusion), channel_id=1, source_target_pairs={{0,1},{1,0},{2,3},{3,2},{4,5},{5,4},{6,7},{7,6},{8,9},{9,8},{10,11... | collective-permute-start | bytes 6291464 | tf_op jit(solution)/shard_map/ppermute | solution.py:360

commit v3 on v2

--- a/solution.py
+++ b/solution.py
@@ -66,7 +66,8 @@
 
     def spans(p):
         rows = shards[p].shape[0]
-        third = rows * 5 // 16 // 16 * 16
+        share = 6 if p < count - 1 else 4
+        third = rows * share // 16 // 16 * 16
         return third, rows - third
 
     def piece(p, owner, own):
@@ -404,11 +405,13 @@
     pieces = share_over_tp(normed_ffn, tp_rank)
     gate_pre = jnp.dot(pieces, gate_w, preferred_element_type=jnp.float32).astype(jnp.bfloat16)
     up_pre = jnp.dot(pieces, up_w, preferred_element_type=jnp.float32).astype(jnp.bfloat16)
+    gate_pre, up_pre = lax.optimization_barrier((gate_pre, up_pre))
     gate_taps = lax.dynamic_slice_in_dim(conv_gate, tp_rank * ff_here, ff_here, 1)
     up_taps = lax.dynamic_slice_in_dim(conv_up, tp_rank * ff_here, ff_here, 1)
     activ = (jax.nn.silu(causal_taps(gate_pre, gate_taps)) * causal_taps(up_pre, up_taps)).astype(
         jnp.bfloat16
     )
+    activ = lax.optimization_barrier(activ)
     ffn_sum = sum_over_tp(
         jnp.dot(activ, down_full, preferred_element_type=jnp.float32).astype(jnp.bfloat16), tp_rank
     )

time: 279 us -> 265 us (0.950)
  matrix products: 48.8 us -> 31.8 us
  other arithmetic: 16.8 us -> 30.8 us
  Pallas kernels: 194 us -> 185 us
    convert_element_type x0 -> x3, other arithmetic: none -> 14 us  [the longest x1 10.7 us: body(): (jax.nn.silu(causal_taps(gate_pre, gate_taps)) * causal_taps(up_pre, up_t...]
    dot_general x1, matrix products: 22.6 us -> 8.68 us  [body(): jnp.dot(activ, down_full, preferred_element_type=jnp.float32)]
    pallas_call x1, Pallas kernels: 194 us -> 185 us  [gather_all(): pl.pallas_call(functools.partial(gather_kernel, sizes, tuple(kinds)), out...]
where the time goes in v3:
time: 265 us
  Pallas kernels  185 us (70%)
  matrix products  31.8 us (12%)
  other arithmetic  30.8 us (12%)
  waiting for transfers between devices  11.7 us (4%)
  local copies, waits for them, and re-layouts  5.09 us (2%)
    pallas_call x1, Pallas kernels, gather_all(): pl.pallas_call(functools.partial(gather_kernel, sizes, tuple(kinds)), out...  185 us
    convert_element_type x1, other arithmetic, body(): (jax.nn.silu(causal_taps(gate_pre, gate_taps)) * causal_taps(up_pre, up_t...  10.7 us
    dot_general x1, matrix products, body(): jnp.dot(pieces, up_w, preferred_element_type=jnp.float32)  8.87 us
    dot_general x1, matrix products, body(): jnp.dot(activ, down_full, preferred_element_type=jnp.float32)  8.68 us
    ppermute x2, waiting for transfers between devices, sum_over_tp(): got = lax.ppermute(theirs, 'tp', [(0, 1), (1, 0)])  8.29 us
    dot_general x1, matrix products, body(): jnp.dot(pieces, gate_w, preferred_element_type=jnp.float32)  7.98 us
    dot_general x1, matrix products, body(): jnp.dot(hidden, out_full, preferred_element_type=jnp.float32)  6.23 us
  transfers between devices with their start and end apart: 3, of which 3 were waited for; matrix products, arithmetic and copies ran while one was open for 0% of the time, Pallas kernels for 0%

profile of v3, /device:TPU:0, one launch (start us, length us, event | category | flops | bytes accessed | tf_op | source)
XLA Modules:
  0.0 265.2 jit_solution(10258655075527402427)
XLA Ops:
  0.0 0.0 copy-start.2
  0.0 0.0 copy-start.1
  0.0 0.0 copy-start
  0.1 2.0 fusion.6
  2.1 0.1 multiply_exponential_fusion
  2.2 0.7 exponential_select_fusion.refs_9_
  2.9 1.3 pad_maximum_fusion.4
  4.2 0.0 copy-done.2
  4.2 0.0 copy-done.1
  4.2 0.0 copy-done
  4.2 0.9 pad_maximum_fusion.3.refs_1_
  5.1 0.8 broadcast_in_dim.24.refs_11_
  5.9 0.8 broadcast_in_dim.23.refs_10_
  6.7 0.6 broadcast_in_dim.25.refs_12_
  7.3 185.2 %shard_map.118 = (bf16[1024,512]{1,0:T(8,128)(2,1)}, bf16[512,2048]{1,0:T(8,128)(2,1)}, bf16[2048,1408]{1,0:T(8,128)(2,1)}, bf16[2048,1408]{1,0:T(8,128)(2,1)}, bf16[1408,2048]{1,0:T(8,128)(2,1)}) custom-call(bf16[512,2048]{1,0:T(8,128)(2,1)} %refs_0_.1, bf16[256,1024]{1,0:T(8,128)(2,1)} %pad_maximum_fusion.3.refs_1_, bf16[512,256]{1,0:T(8,128)(2,1)} %refs_2_.1, ...), custom_call_target="tpu_custom_call" | custom-call | tf_op jit(solution)/shard_map/pallas_call | solution.py:284
  192.5 6.2 %convolution_convert_fusion.3 = bf16[1024,2048]{1,0:T(8,128)(2,1)} fusion(bf16[1024,512]{1,0:T(8,128)(2,1)} %get-tuple-element.12, bf16[512,2048]{1,0:T(8,128)(2,1)} %get-tuple-element.13), kind=kOutput, calls=%fused_computation.13 | convolution fusion | flops 2149580800 | bytes 7340032 | tf_op jit(solution)/shard_map/dot_general | solution.py:400
  198.8 1.7 constant_dynamic-slice_fusion.1
  200.5 0.1 collective-permute-start
  200.6 0.0 copy-start.3
  200.6 4.3 %collective-permute-done = bf16[512,2048]{1,0:T(8,128)(2,1)} collective-permute-done((bf16[512,2048]{1,0:T(8,128)(2,1)S(1)}, bf16[512,2048]{1,0:T(8,128)(2,1)}, u32[]{:S(2)}, u32[]{:S(2)}) %collective-permute-start) | collective-permute-done | bytes 2097184 | tf_op jit(solution)/shard_map/ppermute | solution.py:361
  204.9 4.1 %fusion = (f32[512]{0:T(512)S(1)}, bf16[512,2048]{1,0:T(8,128)(2,1)S(1)}) fusion(bf16[512,2048]{1,0:T(8,128)(2,1)} %collective-permute-done, bf16[1024,2048]{1,0:T(8,128)(2,1)} %convolution_convert_fusion.3, s32[]{:T(128)S(6)} %select_n.29, bf16[512,2048]{1,0:T(8,128)(2,1)} %refs_0_.1), kind=kLoop, calls=%fused_computation.4 | loop fusion | flops 9436672 | bytes 8390660 | tf_op jit(solution)/shard_map/reduce_sum | solution.py:312
  209.0 0.0 copy-done.3
  209.0 1.9 fusion.2
  210.9 0.1 collective-permute-start.1
  211.0 1.0 dynamic-slice_reduce_fusion.2
  212.0 3.4 %collective-permute-done.1 = bf16[512,2048]{1,0:T(8,128)(2,1)} collective-permute-done((bf16[512,2048]{1,0:T(8,128)(2,1)}, bf16[512,2048]{1,0:T(8,128)(2,1)}, u32[]{:S(2)}, u32[]{:S(2)}) %collective-permute-start.1) | collective-permute-done | bytes 2097184 | tf_op jit(solution)/shard_map/ppermute | solution.py:366
  215.4 0.0 slice-start
  215.4 3.2 %broadcast_select_fusion.1 = (bf16[512,2048]{1,0:T(8,128)(2,1)S(1)}, bf16[512,2048]{1,0:T(8,128)(2,1)S(1)}) fusion(bf16[512,2048]{1,0:T(8,128)(2,1)} %collective-permute-done.1, pred[]{:T(512)S(6)} %eq.3, f32[2048]{0:T(1024)S(1)} %copy-done.3, f32[512]{0:T(512)S(1)} %add_rsqrt_fusion, bf16[512,2048]{1,0:T(8,128)(2,1)S(1)} %get-tuple-element.26), kind=kLoop, calls=%fused_computation.15 | loop fusion | flops 6291456 | bytes 8398849 | tf_op jit(solution)/shard_map/jit(_where)/select_n | solution.py:368
  218.6 0.0 slice-start.1
  218.6 8.9 %convolution_convert_fusion = bf16[1024,1408]{1,0:T(8,128)(2,1)S(1)} fusion(bf16[2048,1408]{1,0:T(8,128)(2,1)} %get-tuple-element.15, bf16[512,2048]{1,0:T(8,128)(2,1)S(1)} %get-tuple-element.28, bf16[512,2048]{1,0:T(8,128)(2,1)S(1)} %get-tuple-element.27), kind=kOutput, calls=%fused_computation.10 | convolution fusion | flops 5915410432 | bytes 12845056 | tf_op jit(solution)/shard_map/dot_general | solution.py:407
  227.5 0.0 slice-done
  227.5 0.0 slice-done.1
  227.5 8.0 %convolution_convert_fusion.1 = bf16[1024,1408]{1,0:T(8,128)(2,1)S(1)} fusion(bf16[2048,1408]{1,0:T(8,128)(2,1)S(1)} %bitcast.9, bf16[512,2048]{1,0:T(8,128)(2,1)S(1)} %get-tuple-element.28, bf16[512,2048]{1,0:T(8,128)(2,1)S(1)} %get-tuple-element.27), kind=kOutput, calls=%fused_computation.11 | convolution fusion | flops 5915410432 | bytes 12845056 | tf_op jit(solution)/shard_map/dot_general | solution.py:406
  235.5 0.4 convert_element_type.71
  235.9 2.9 %convert_element_type.72 = f32[1024,1408]{1,0:T(8,128)} convert(bf16[1024,1408]{1,0:T(8,128)(2,1)S(1)} %convolution_convert_fusion) | non-fusion elementwise | flops 1441792 | bytes 8650752 | tf_op jit(solution)/shard_map/convert_element_type | solution.py:350
  238.8 10.7 %multiply_convert_fusion = bf16[1024,1408]{1,0:T(8,128)(2,1)S(1)} fusion(f32[1024,1408]{1,0:T(8,128)} %convert_element_type.72, f32[1024,1408]{1,0:T(8,128)S(1)} %convert_element_type.71, f32[1408]{0:T(1024)S(1)} %get-tuple-element.24, f32[1408]{0:T(1024)S(1)} %get-tuple-element.23, f32[1408]{0:T(1024)S(1)} %get-tuple-element.22, ...), kind=kLoop, calls=%fused_computation.3 | loop fusion | flops 23068672 | bytes 14451712 | tf_op jit(solution)/shard_map/convert_element_type | solution.py:411
  249.5 8.7 %convolution_convert_fusion.2 = bf16[1024,2048]{1,0:T(8,128)(2,1)S(1)} fusion(bf16[1024,1408]{1,0:T(8,128)(2,1)S(1)} %multiply_convert_fusion, bf16[1408,2048]{1,0:T(8,128)(2,1)} %get-tuple-element.18), kind=kOutput, calls=%fused_computation.12 | convolution fusion | flops 5907677184 | bytes 12845056 | tf_op jit(solution)/shard_map/dot_general | solution.py:416
  258.2 0.1 constant_dynamic-slice_fusion
  258.4 0.2 collective-permute-start.2
  258.6 4.0 %collective-permute-done.2 = bf16[512,2048]{1,0:T(8,128)(2,1)S(1)} collective-permute-done((bf16[512,2048]{1,0:T(8,128)(2,1)S(1)}, bf16[512,2048]{1,0:T(8,128)(2,1)S(1)}, u32[]{:S(2)}, u32[]{:S(2)}) %collective-permute-start.2) | collective-permute-done | bytes 2097184 | tf_op jit(solution)/shard_map/ppermute | solution.py:361
  262.6 2.6 fusion.3
  (7 shorter events, 0.1 us)
Async XLA Ops:
  0.0 4.2 %copy-start.2 = (bf16[256,256]{1,0:T(8,128)(2,1)S(1)}, bf16[256,256]{1,0:T(8,128)(2,1)}, u32[]{:S(2)}) copy-start(bf16[256,256]{1,0:T(8,128)(2,1)} %param.14) | copy-start | bytes 393220
  0.0 4.2 %copy-start.1 = (bf16[256,256]{1,0:T(8,128)(2,1)S(1)}, bf16[256,256]{1,0:T(8,128)(2,1)}, u32[]{:S(2)}) copy-start(bf16[256,256]{1,0:T(8,128)(2,1)} %param.15) | copy-start | bytes 393220
  0.0 4.2 %copy-start = (bf16[256,512]{1,0:T(8,128)(2,1)S(1)}, bf16[256,512]{1,0:T(8,128)(2,1)}, u32[]{:S(2)}) copy-start(bf16[256,512]{1,0:T(8,128)(2,1)} %param.16) | copy-start | bytes 786436
  200.5 4.4 %collective-permute-start = (bf16[512,2048]{1,0:T(8,128)(2,1)S(1)}, bf16[512,2048]{1,0:T(8,128)(2,1)}, u32[]{:S(2)}, u32[]{:S(2)}) collective-permute-start(bf16[512,2048]{1,0:T(8,128)(2,1)S(1)} %constant_dynamic-slice_fusion.1), channel_id=1, source_target_pairs={{0,1},{1,0},{2,3},{3,2},{4,5},{5,4},{6,7},{7,6},{8,9},{9,8},{10,11... | collective-permute-start | bytes 6291464 | tf_op jit(solution)/shard_map/ppermute | solution.py:361
  200.6 8.4 %copy-start.3 = (f32[2048]{0:T(1024)S(1)}, f32[2048]{0:T(1024)}, u32[]{:S(2)}) copy-start(f32[2048]{0:T(1024)} %param.18) | copy-start | bytes 24580
  210.9 4.5 %collective-permute-start.1 = (bf16[512,2048]{1,0:T(8,128)(2,1)}, bf16[512,2048]{1,0:T(8,128)(2,1)}, u32[]{:S(2)}, u32[]{:S(2)}) collective-permute-start(bf16[512,2048]{1,0:T(8,128)(2,1)} %fusion.2), channel_id=1, source_target_pairs={{0,1},{1,0},{2,3},{3,2},{4,5},{5,4},{6,7},{7,6},{8,9},{9,8},{10,11... | collective-permute-start | bytes 6291464 | tf_op jit(solution)/shard_map/ppermute | solution.py:366
  215.4 12.1 %slice-start = ((s8[5767168]{0:T(1024)(128)(4,1)}), s8[4194304]{0:T(1024)(128)(4,1)S(1)}, s32[]{:S(2)}) async-start(s8[5767168]{0:T(1024)(128)(4,1)} %bitcast.8), calls=%async_computation | async-start | bytes 8388608
  218.6 8.9 %slice-start.1 = ((s8[5767168]{0:T(1024)(128)(4,1)}), s8[1572864]{0:T(1024)(128)(4,1)S(1)}, s32[]{:S(2)}) async-start(s8[5767168]{0:T(1024)(128)(4,1)} %bitcast.8), calls=%async_computation.1 | async-start | bytes 3145728
  258.4 4.2 %collective-permute-start.2 = (bf16[512,2048]{1,0:T(8,128)(2,1)S(1)}, bf16[512,2048]{1,0:T(8,128)(2,1)S(1)}, u32[]{:S(2)}, u32[]{:S(2)}) collective-permute-start(bf16[512,2048]{1,0:T(8,128)(2,1)S(1)} %constant_dynamic-slice_fusion), channel_id=1, source_target_pairs={{0,1},{1,0},{2,3},{3,2},{4,5},{5,4},{6,7},{7,6},{8,9},{9,8},{10,11... | collective-permute-start | bytes 6291464 | tf_op jit(solution)/shard_map/ppermute | solution.py:361
